TPU v7x, 512 devices: a 4x2x32 block of a 4x8x32 slice. The times are simulated.
512 devices in a mesh: grp: 2 (over y), sp: 64 (over z, core), tp: 4 (over x).
Axes of the slice: x: 4, y: 2, z: 32, core: 2. Of those that a mesh axis runs over, the one named last changes fastest.
The devices are a block of a 4x8x32 slice.
Arguments:
- hidden: bfloat16 [49152, 2048], P(('grp', 'sp'), 'tp'), parts along dimension 0, may hold values from -45 to 45
- norm_gain: bfloat16 [2048], replicated, may hold values from 0.099609375 to 1.8984375
- w_query: bfloat16 [2048, 1024], P(None, 'tp'), may hold values from -0.125 to 0.125
- w_key: bfloat16 [2048, 1024], P(None, 'tp'), may hold values from -0.125 to 0.125
- w_value: bfloat16 [2048, 1024], P(None, 'tp'), may hold values from -0.125 to 0.125
- query_gain: float32 [8, 128], P('tp'), may hold values from 0.3 to 16
- key_gain: float32 [8, 128], P('tp'), may hold values from 0.3 to 16
- w_out: bfloat16 [1024, 2048], P('tp'), may hold values from -1.5 to 1.5
Outputs:
- mixed: bfloat16 [49152, 2048], P(('grp', 'sp'), 'tp'), parts along dimension 0
- log_total: float32 [49152, 8], P(('grp', 'sp'), 'tp'), parts along dimension 0
There are 2 independent parts, one for each index of `grp`. A program takes and returns all parts, laid end to end along the dimension named above; an argument that names none is the same for every part. Nothing has to cross between parts.
All inputs are finite; a program needn't handle non-finite values.
Results may differ from a plain program's by a relative error of at most 0.015.
The roundings to bfloat16 on the way count: a program that leaves them out, or rounds other values in their place, can miss the bound.
Values may be sent and summed in bfloat16 or wider, within the bound.
A program may use at most 64 MiB of HBM per device.

v0:
```python
import math

import jax
import jax.numpy as jnp
from jax import lax
from jax.sharding import PartitionSpec as P

D = 2048
KEYS_BEHIND = 128
MIDDLE_DILATION = 4
WIDEST_DILATION = 16


EPSILON = 1e-06
ROTARY_BASE = 500000.0


def from_behind(value, axis, steps):
    count = lax.axis_size(axis)
    initial, last = (max(0, -steps), min(count, count - steps))
    return lax.ppermute(value, axis, [(source, source + steps) for source in range(initial, last)])


def in_order(blocks, dim):
    blocks = jnp.moveaxis(blocks, 0, dim)
    shape = blocks.shape
    return blocks.reshape(*shape[:dim], shape[dim] * shape[dim + 1], *shape[dim + 2 :])


def sent_to_all(shard, axis):
    length = lax.axis_size(axis)
    return lax.all_to_all(
        jnp.broadcast_to(shard[None], (length, *shard.shape)), axis, 0, 0, tiled=True
    )


def gathered_copies(shard, axis, dim):
    return in_order(sent_to_all(shard, axis), dim)


def rotate(values, positions):
    head_width = values.shape[-1]
    inverse = ROTARY_BASE ** (-jnp.arange(0, head_width, 2, dtype=jnp.float32) / head_width)
    angles = positions[:, None] * inverse[None, :]
    cosine = jnp.cos(angles)[:, None, :]
    sine = jnp.sin(angles)[:, None, :]
    half_width = head_width // 2
    first_half = values[..., :half_width]
    second_half = values[..., half_width:]
    return jnp.concatenate(
        [first_half * cosine - second_half * sine, second_half * cosine + first_half * sine],
        axis=-1,
    )


def head_norm(values, gains):
    normed = values * lax.rsqrt(jnp.mean(values * values, axis=-1, keepdims=True) + EPSILON)
    return normed * gains[None, :, :]


def earlier_pairs(own_pair, token_rows):
    distant_shards = (KEYS_BEHIND * WIDEST_DILATION + token_rows - 1) // token_rows
    buffer = own_pair
    shards = 1
    while shards < distant_shards + 1:
        needed = min(shards, distant_shards + 1 - shards)
        outgoing = buffer[:, buffer.shape[1] - needed * token_rows :]
        arrived = from_behind(outgoing, "sp", shards)
        buffer = jnp.concatenate([arrived, buffer], axis=1)
        shards = shards + needed
    return buffer


def local_branch(query, key_rows, value_rows, dilation_step, first_pos):
    token_rows, head_count, head_width = query.shape
    reach_rows = KEYS_BEHIND * dilation_step
    buffer_rows = key_rows.shape[0]
    class_rows = token_rows // dilation_step
    class_keys = class_rows + KEYS_BEHIND
    window_start = buffer_rows - token_rows - reach_rows
    key_window = key_rows[window_start:]
    value_window = value_rows[window_start:]
    query_class = query.reshape(class_rows, dilation_step, head_count, head_width).transpose(
        1, 0, 2, 3
    )
    key_class = key_window.reshape(class_keys, dilation_step, head_count, head_width).transpose(
        1, 0, 2, 3
    )
    value_class = value_window.reshape(class_keys, dilation_step, head_count, head_width).transpose(
        1, 0, 2, 3
    )
    block_rows = math.gcd(class_rows, KEYS_BEHIND) if class_rows > KEYS_BEHIND else class_rows
    block_count = class_rows // block_rows
    query_blocks = query_class.reshape(
        dilation_step, block_count, block_rows, head_count, head_width
    )
    key_blocks = jnp.stack(
        [
            key_class[:, number * block_rows : number * block_rows + block_rows + KEYS_BEHIND]
            for number in range(block_count)
        ],
        axis=1,
    )
    value_blocks = jnp.stack(
        [
            value_class[:, number * block_rows : number * block_rows + block_rows + KEYS_BEHIND]
            for number in range(block_count)
        ],
        axis=1,
    )
    scores = jnp.einsum(
        "rnqhd,rnkhd->rnhqk", query_blocks, key_blocks, preferred_element_type=jnp.float32
    ) * head_width ** (-0.5)
    row_index = jnp.arange(block_rows, dtype=jnp.int32)[:, None]
    col_index = jnp.arange(block_rows + KEYS_BEHIND, dtype=jnp.int32)[None, :]
    distance = KEYS_BEHIND + row_index - col_index
    in_band = (distance >= 0) & (distance <= KEYS_BEHIND)
    class_index = jnp.arange(block_count, dtype=jnp.int32)[:, None] * block_rows + col_index
    residue = jnp.arange(dilation_step, dtype=jnp.int32)[:, None, None]
    key_position = first_pos - reach_rows + class_index[None] * dilation_step + residue
    allowed = in_band[None, None, None, :, :] & (key_position >= 0)[:, :, None, None, :]
    scores = jnp.where(allowed, scores, -jnp.inf)
    row_max = jnp.max(scores, axis=-1, keepdims=True)
    weights = jnp.exp(scores - row_max)
    weight_sum = jnp.sum(weights, axis=-1)
    weighted = jnp.einsum(
        "rnhqk,rnkhd->rnqhd",
        weights.astype(jnp.bfloat16),
        value_blocks,
        preferred_element_type=jnp.float32,
    )
    branch_out = weighted / jnp.transpose(weight_sum, (0, 1, 3, 2))[..., None]
    branch_out = branch_out.reshape(dilation_step, class_rows, head_count, head_width).transpose(
        1, 0, 2, 3
    )
    branch_out = branch_out.reshape(token_rows, head_count, head_width)
    log_sum = jnp.transpose(row_max[..., 0] + jnp.log(weight_sum), (0, 1, 3, 2))
    log_sum = (
        log_sum.reshape(dilation_step, class_rows, head_count)
        .transpose(1, 0, 2)
        .reshape(token_rows, head_count)
    )
    return (branch_out, log_sum)


def local(hidden, norm_gain, w_query, w_key, w_value, query_gain, key_gain, w_out):
    token_rows = hidden.shape[0]
    local_width = w_query.shape[1]
    head_count = query_gain.shape[0]
    head_width = query_gain.shape[1]
    gain_full = norm_gain.astype(jnp.float32)
    raw_piece = gathered_copies(hidden, "tp", 1).astype(jnp.float32)
    scaled = (raw_piece * gain_full[None, :]).astype(jnp.bfloat16)

    def add_product(weight):
        return jnp.dot(scaled, weight, preferred_element_type=jnp.float32)

    query_raw = add_product(w_query)
    key_raw = add_product(w_key)
    value_raw = add_product(w_value)
    squares = jnp.sum(raw_piece * raw_piece, axis=1)
    row_scale = lax.rsqrt(squares / D + EPSILON)[:, None]
    first_pos = lax.axis_index("sp") * token_rows
    positions = (jnp.arange(token_rows, dtype=jnp.int32) + first_pos).astype(jnp.float32)
    query = rotate(
        head_norm((query_raw * row_scale).reshape(token_rows, head_count, head_width), query_gain),
        positions,
    ).astype(jnp.bfloat16)
    key_now = rotate(
        head_norm((key_raw * row_scale).reshape(token_rows, head_count, head_width), key_gain),
        positions,
    ).astype(jnp.bfloat16)
    value_now = (value_raw * row_scale).astype(jnp.bfloat16)
    own_pair = jnp.stack([key_now.reshape(token_rows, local_width), value_now], axis=0)
    buffer = earlier_pairs(own_pair, token_rows)
    key_rows = buffer[0].reshape(-1, head_count, head_width)
    value_rows = buffer[1].reshape(-1, head_count, head_width)
    branch_outs = []
    branch_logs = []
    for dilation_step in (1, MIDDLE_DILATION, WIDEST_DILATION):
        branch_out, log_sum = local_branch(query, key_rows, value_rows, dilation_step, first_pos)
        branch_outs.append(branch_out)
        branch_logs.append(log_sum)
    stacked_logs = jnp.stack(branch_logs, axis=0)
    peak = jnp.max(stacked_logs, axis=0)
    log_total = peak + jnp.log(jnp.sum(jnp.exp(stacked_logs - peak[None]), axis=0))
    shares = jnp.exp(stacked_logs - log_total[None])
    attended = jnp.sum(shares[..., None] * jnp.stack(branch_outs, axis=0), axis=0)
    attended = attended.astype(jnp.bfloat16).reshape(token_rows, local_width)
    column_block = lax.all_to_all(w_out, "tp", split_axis=1, concat_axis=0, tiled=True)
    mixed = jnp.dot(
        gathered_copies(attended, "tp", 1), column_block, preferred_element_type=jnp.float32
    )
    return (mixed.astype(jnp.bfloat16), log_total)


def solution(mesh):
    placed = (
        P(("grp", "sp"), "tp"),
        P(),
        P(None, "tp"),
        P(None, "tp"),
        P(None, "tp"),
        P("tp", None),
        P("tp", None),
        P("tp", None),
    )
    return jax.shard_map(
        local,
        mesh=mesh,
        in_specs=placed,
        out_specs=(P(("grp", "sp"), "tp"), P(("grp", "sp"), "tp")),
        check_vma=False,
    )
```

profile of v0, /device:TPU:96, one launch (start us, length us, event | category | flops | bytes accessed | tf_op | source)
XLA Modules:
  0.0 177.7 jit_solution(3688576137176458668)
XLA Ops:
  3.3 4.7 %all-to-all-start = ((bf16[4,384,512]{1,2,0:T(8,128)(2,1)}), bf16[4,384,512]{1,2,0:T(8,128)(2,1)S(1)}, u32[]{:S(2)}, u32[]{:S(2)}) async-start(bf16[4,384,512]{1,2,0:T(8,128)(2,1)} %broadcast_in_dim.33), calls=%async_computation | async-start | bytes 3145728 | tf_op jit(solution)/shard_map/all_to_all | solution.py:32
  8.2 2.3 %copy.136 = bf16[256,2048]{0,1:T(8,128)(2,1)} copy(bf16[256,2048]{1,0:T(8,128)(2,1)} %param.15) | data formatting | bytes 2097152 | tf_op args[7]
  10.5 2.3 %copy.137 = bf16[256,4,512]{2,0,1:T(8,128)(2,1)} copy(bf16[256,4,512]{0,2,1:T(8,128)(2,1)} %bitcast.194) | data formatting | bytes 2097152 | tf_op jit(solution)/shard_map/all_to_all | solution.py:190
  15.1 13.7 %all-to-all-done = bf16[4,384,512]{1,2,0:T(8,128)(2,1)S(1)} async-done(((bf16[4,384,512]{1,2,0:T(8,128)(2,1)}), bf16[4,384,512]{1,2,0:T(8,128)(2,1)S(1)}, u32[]{:S(2)}, u32[]{:S(2)}) %all-to-all-start) | async-done | bytes 1572896 | tf_op jit(solution)/shard_map/all_to_all | solution.py:32
  28.8 4.3 %all-to-all-start.2 = ((bf16[256,4,512]{2,0,1:T(8,128)(2,1)}), bf16[256,4,512]{2,0,1:T(8,128)(2,1)}, u32[]{:S(2)}, u32[]{:S(2)}) async-start(bf16[256,4,512]{2,0,1:T(8,128)(2,1)} %copy.137), calls=%async_computation.2 | async-start | bytes 2097152 | tf_op jit(solution)/shard_map/all_to_all | solution.py:190
  39.3 2.0 %collective-permute-start = (bf16[2,384,256]{1,2,0:T(8,128)(2,1)S(1)}, bf16[2,384,256]{1,2,0:T(8,128)(2,1)S(1)}, u32[]{:S(2)}, u32[]{:S(2)}) collective-permute-start(bf16[2,384,256]{1,2,0:T(8,128)(2,1)S(1)} %pad_maximum_fusion.3), channel_id=1, source_target_pairs={{0,4},{4,8},{8,12},{12,16},{16,20},{20,24},{24,28},{28,32},{32,36}... | collective-permute-start | bytes 1179656 | tf_op jit(solution)/shard_map/ppermute | solution.py:21
  44.9 3.5 %collective-permute-done = bf16[2,384,256]{1,2,0:T(8,128)(2,1)S(1)} collective-permute-done((bf16[2,384,256]{1,2,0:T(8,128)(2,1)S(1)}, bf16[2,384,256]{1,2,0:T(8,128)(2,1)S(1)}, u32[]{:S(2)}, u32[]{:S(2)}) %collective-permute-start) | collective-permute-done | bytes 393248 | tf_op jit(solution)/shard_map/ppermute | solution.py:21
  49.2 4.7 %collective-permute-start.1 = (bf16[2,768,256]{1,2,0:T(8,128)(2,1)S(1)}, bf16[2,768,256]{1,2,0:T(8,128)(2,1)S(1)}, u32[]{:S(2)}, u32[]{:S(2)}) collective-permute-start(bf16[2,768,256]{1,2,0:T(8,128)(2,1)S(1)} %maximum_maximum_fusion.2), channel_id=1, source_target_pairs={{0,8},{4,12},{8,16},{12,20},{16,24},{20,28},{24,32},{28,36},{32,40... | collective-permute-start | bytes 2359304 | tf_op jit(solution)/shard_map/ppermute | solution.py:21
  54.7 1.7 copy.144
  56.3 1.6 copy.145
  58.7 1.8 fusion.78
  60.5 1.7 copy.147
  62.1 1.7 copy.148
  64.6 1.7 fusion.82
  68.0 25.2 %collective-permute-done.1 = bf16[2,768,256]{1,2,0:T(8,128)(2,1)S(1)} collective-permute-done((bf16[2,768,256]{1,2,0:T(8,128)(2,1)S(1)}, bf16[2,768,256]{1,2,0:T(8,128)(2,1)S(1)}, u32[]{:S(2)}, u32[]{:S(2)}) %collective-permute-start.1) | collective-permute-done | bytes 786464 | tf_op jit(solution)/shard_map/ppermute | solution.py:21
  94.5 2.3 %collective-permute-start.2 = (bf16[2,1152,256]{1,2,0:T(8,128)(2,1)}, bf16[2,1152,256]{1,2,0:T(8,128)(2,1)}, u32[]{:S(2)}, u32[]{:S(2)}) collective-permute-start(bf16[2,1152,256]{1,2,0:T(8,128)(2,1)} %slice.94), channel_id=1, source_target_pairs={{0,16},{4,20},{8,24},{12,28},{16,32},{20,36},{24,40},{28,44},{32,4... | collective-permute-start | bytes 3538952 | tf_op jit(solution)/shard_map/ppermute | solution.py:21
  99.6 1.6 fusion.81
  106.5 37.0 %collective-permute-done.2 = bf16[2,1152,256]{1,2,0:T(8,128)(2,1)} collective-permute-done((bf16[2,1152,256]{1,2,0:T(8,128)(2,1)}, bf16[2,1152,256]{1,2,0:T(8,128)(2,1)}, u32[]{:S(2)}, u32[]{:S(2)}) %collective-permute-start.2) | collective-permute-done | bytes 1179680 | tf_op jit(solution)/shard_map/ppermute | solution.py:21
  143.4 2.6 %maximum_maximum_fusion.1 = (bf16[1,2432,256]{1,2,0:T(8,128)(2,1)}, bf16[1,2432,256]{1,2,0:T(8,128)(2,1)}) fusion(bf16[1,384,256]{1,2,0:T(8,128)(2,1)S(1)} %fusion.16, bf16[1,384,256]{1,2,0:T(8,128)(2,1)S(1)} %bitcast.193, bf16[2,384,256]{1,2,0:T(8,128)(2,1)S(1)} %collective-permute-done, bf16[2,768,256]{1,2,0:T(8,128)(2,1)S(1)} %collective-permute-done.1, ...), kind=kLoop, calls=%fused_computation.16 | loop fusion | flops 12451840 | bytes 5242880 | tf_op jit(solution)/shard_map/slice | solution.py:81
  146.0 1.7 copy.119
  148.1 2.1 %fusion.80 = (f32[16,2,24]{2,1,0:T(2,128)S(1)}, f32[16,2,24,152]{3,2,1,0:T(8,128)S(1)}) fusion(bf16[152,16,2,128]{3,2,1,0:T(2,128)(2,1)S(1)} %reshape.545, bf16[24,16,2,64]{3,0,2,1:T(8,128)(2,1)} %copy.118, bf16[24,16,2,64]{3,0,2,1:T(8,128)(2,1)} %copy.117, pred[16,24,152]{2,1,0:T(8,128)(4,1)} %broadcast_and_fusion), kind=kOutput, calls=%fused_computation.139 | convolution fusion | flops 30627072 | bytes 1970176 | tf_op jit(solution)/shard_map/rnqhd,rnkhd->rnhqk/dot_general | solution.py:111
  154.9 2.1 %fusion.24 = f32[24,16,2,128]{3,0,2,1:T(8,128)S(1)} fusion(bf16[152,16,2,128]{3,2,1,0:T(2,128)(2,1)} %reshape.550, f32[16,2,24,152]{3,2,1,0:T(8,128)S(1)} %copy-done.3, f32[16,2,24]{2,1,0:T(2,128)S(1)} %get-tuple-element.26, f32[16,24,2]{1,2,0:T(2,128)} %bitcast.215), kind=kOutput, calls=%fused_computation.37 | convolution fusion | flops 30216192 | bytes 2111488 | tf_op jit(solution)/shard_map/rnhqk,rnkhd->rnqhd/dot_general | solution.py:126
  158.2 17.0 %all_to_all.26 = bf16[4,384,256]{2,1,0:T(8,128)(2,1)S(1)} all-to-all(bf16[4,384,256]{2,1,0:T(8,128)(2,1)S(1)} %broadcast_in_dim.39), channel_id=1, replica_groups=mesh['grp'=2,'sp'=64,'tp'=4] {'tp'}, dimensions={0} | all-to-all | bytes 1572864 | tf_op jit(solution)/shard_map/all_to_all | solution.py:32
  175.2 2.5 %fusion.4 = bf16[384,512]{1,0:T(8,128)(2,1)} fusion(bf16[256,4,512]{2,0,1:T(8,128)(2,1)} %all-to-all-done.2, bf16[4,384,256]{2,1,0:T(8,128)(2,1)S(1)} %all_to_all.26), kind=kOutput, calls=%fused_computation.11 | convolution fusion | flops 402849792 | bytes 2228224 | tf_op jit(solution)/shard_map/dot_general | solution.py:191
  (139 shorter events, 34.8 us)
Async XLA Ops:
  0.6 34.9 %copy-start = (bf16[2048,256]{1,0:T(8,128)(2,1)S(1)}, bf16[2048,256]{1,0:T(8,128)(2,1)}, u32[]{:S(2)}) copy-start(bf16[2048,256]{1,0:T(8,128)(2,1)} %param.11) | copy-start | bytes 3145732
  3.3 4.9 %copy-start.24 = (bf16[2048]{0:T(1024)(128)(2,1)S(1)}, bf16[2048]{0:T(1024)(128)(2,1)}, u32[]{:S(2)}) copy-start(bf16[2048]{0:T(1024)(128)(2,1)} %param.9) | copy-start | bytes 12292
  3.3 25.5 %all-to-all-start = ((bf16[4,384,512]{1,2,0:T(8,128)(2,1)}), bf16[4,384,512]{1,2,0:T(8,128)(2,1)S(1)}, u32[]{:S(2)}, u32[]{:S(2)}) async-start(bf16[4,384,512]{1,2,0:T(8,128)(2,1)} %broadcast_in_dim.33), calls=%async_computation | async-start | bytes 3145728 | tf_op jit(solution)/shard_map/all_to_all | solution.py:32
  28.8 129.4 %all-to-all-start.2 = ((bf16[256,4,512]{2,0,1:T(8,128)(2,1)}), bf16[256,4,512]{2,0,1:T(8,128)(2,1)}, u32[]{:S(2)}, u32[]{:S(2)}) async-start(bf16[256,4,512]{2,0,1:T(8,128)(2,1)} %copy.137), calls=%async_computation.2 | async-start | bytes 2097152 | tf_op jit(solution)/shard_map/all_to_all | solution.py:190
  38.9 6.0 %copy-start.4 = (bf16[384,2,64]{2,0,1:T(8,128)(2,1)}, bf16[384,2,64]{2,0,1:T(8,128)(2,1)S(1)}, u32[]{:S(2)}) copy-start(bf16[384,2,64]{2,0,1:T(8,128)(2,1)S(1)} %get-tuple-element.8) | copy-start | bytes 294916
  38.9 6.0 %copy-start.5 = (bf16[384,2,64]{2,0,1:T(8,128)(2,1)}, bf16[384,2,64]{2,0,1:T(8,128)(2,1)S(1)}, u32[]{:S(2)}) copy-start(bf16[384,2,64]{2,0,1:T(8,128)(2,1)S(1)} %get-tuple-element.9) | copy-start | bytes 294916
  39.3 9.1 %collective-permute-start = (bf16[2,384,256]{1,2,0:T(8,128)(2,1)S(1)}, bf16[2,384,256]{1,2,0:T(8,128)(2,1)S(1)}, u32[]{:S(2)}, u32[]{:S(2)}) collective-permute-start(bf16[2,384,256]{1,2,0:T(8,128)(2,1)S(1)} %pad_maximum_fusion.3), channel_id=1, source_target_pairs={{0,4},{4,8},{8,12},{12,16},{16,20},{20,24},{24,28},{28,32},{32,36}... | collective-permute-start | bytes 1179656 | tf_op jit(solution)/shard_map/ppermute | solution.py:21
  49.2 44.0 %collective-permute-start.1 = (bf16[2,768,256]{1,2,0:T(8,128)(2,1)S(1)}, bf16[2,768,256]{1,2,0:T(8,128)(2,1)S(1)}, u32[]{:S(2)}, u32[]{:S(2)}) collective-permute-start(bf16[2,768,256]{1,2,0:T(8,128)(2,1)S(1)} %maximum_maximum_fusion.2), channel_id=1, source_target_pairs={{0,8},{4,12},{8,16},{12,20},{16,24},{20,28},{24,32},{28,36},{32,40... | collective-permute-start | bytes 2359304 | tf_op jit(solution)/shard_map/ppermute | solution.py:21
  64.6 2.0 %copy-start.11 = (bf16[1,256,2,128]{3,1,2,0:T(8,128)(2,1)S(1)}, bf16[1,256,2,128]{3,1,2,0:T(8,128)(2,1)}, u32[]{:S(2)}) copy-start(bf16[1,256,2,128]{3,1,2,0:T(8,128)(2,1)} %copy.147) | copy-start | bytes 393220
  64.6 2.0 %copy-start.12 = (bf16[1,256,2,128]{3,1,2,0:T(8,128)(2,1)S(1)}, bf16[1,256,2,128]{3,1,2,0:T(8,128)(2,1)}, u32[]{:S(2)}) copy-start(bf16[1,256,2,128]{3,1,2,0:T(8,128)(2,1)} %copy.148) | copy-start | bytes 393220
  64.6 2.0 %copy-start.13 = (bf16[1,256,2,128]{3,1,2,0:T(8,128)(2,1)S(1)}, bf16[1,256,2,128]{3,1,2,0:T(8,128)(2,1)}, u32[]{:S(2)}) copy-start(bf16[1,256,2,128]{3,1,2,0:T(8,128)(2,1)} %copy.149) | copy-start | bytes 393220
  66.3 30.5 %copy-start.15 = (f32[3,2,128]{2,1,0:T(2,128)}, f32[3,2,128]{2,1,0:T(2,128)S(1)}, u32[]{:S(2)}) copy-start(f32[3,2,128]{2,1,0:T(2,128)S(1)} %get-tuple-element.30) | copy-start | bytes 9220
  66.6 30.2 %copy-start.17 = (f32[3,2,128]{2,1,0:T(2,128)}, f32[3,2,128]{2,1,0:T(2,128)S(1)}, u32[]{:S(2)}) copy-start(f32[3,2,128]{2,1,0:T(2,128)S(1)} %fusion.29) | copy-start | bytes 9220
  94.5 49.0 %collective-permute-start.2 = (bf16[2,1152,256]{1,2,0:T(8,128)(2,1)}, bf16[2,1152,256]{1,2,0:T(8,128)(2,1)}, u32[]{:S(2)}, u32[]{:S(2)}) collective-permute-start(bf16[2,1152,256]{1,2,0:T(8,128)(2,1)} %slice.94), channel_id=1, source_target_pairs={{0,16},{4,20},{8,24},{12,28},{16,32},{20,36},{24,40},{28,44},{32,4... | collective-permute-start | bytes 3538952 | tf_op jit(solution)/shard_map/ppermute | solution.py:21
  148.1 4.7 %copy-start.1 = (bf16[1,2432,256]{1,2,0:T(8,128)(2,1)S(1)}, bf16[1,2432,256]{1,2,0:T(8,128)(2,1)}, u32[]{:S(2)}) copy-start(bf16[1,2432,256]{1,2,0:T(8,128)(2,1)} %get-tuple-element.3) | copy-start | bytes 3735556
  154.9 2.2 %copy-start.16 = (f32[3,2,128]{2,1,0:T(2,128)S(1)}, f32[3,2,128]{2,1,0:T(2,128)}, u32[]{:S(2)}) copy-start(f32[3,2,128]{2,1,0:T(2,128)} %copy-done.15) | copy-start | bytes 9220
  154.9 2.2 %copy-start.18 = (f32[3,2,128]{2,1,0:T(2,128)S(1)}, f32[3,2,128]{2,1,0:T(2,128)}, u32[]{:S(2)}) copy-start(f32[3,2,128]{2,1,0:T(2,128)} %copy-done.17) | copy-start | bytes 9220
  154.9 2.2 %copy-start.21 = (f32[384,2]{0,1:T(2,128)S(1)}, f32[384,2]{0,1:T(2,128)}, u32[]{:S(2)}) copy-start(f32[384,2]{0,1:T(2,128)} %stack_reshape.13) | copy-start | bytes 9220
  154.9 2.2 %copy-start.22 = (f32[384,2]{0,1:T(2,128)S(1)}, f32[384,2]{0,1:T(2,128)}, u32[]{:S(2)}) copy-start(f32[384,2]{0,1:T(2,128)} %stack_reshape.14) | copy-start | bytes 9220
  154.9 2.2 %copy-start.10 = (f32[24,16,2]{1,0,2:T(8,128)S(1)}, f32[24,16,2]{1,0,2:T(8,128)}, u32[]{:S(2)}) copy-start(f32[24,16,2]{1,0,2:T(8,128)} %copy-done.9) | copy-start | bytes 9220
  154.9 2.4 %copy-start.19 = (f32[1,384,2]{1,2,0:T(2,128)S(1)}, f32[1,384,2]{1,2,0:T(2,128)}, u32[]{:S(2)}) copy-start(f32[1,384,2]{1,2,0:T(2,128)} %stack.53) | copy-start | bytes 9220
  154.9 2.4 %copy-start.20 = (f32[1,384,2]{1,2,0:T(2,128)S(1)}, f32[1,384,2]{1,2,0:T(2,128)}, u32[]{:S(2)}) copy-start(f32[1,384,2]{1,2,0:T(2,128)} %fusion.76) | copy-start | bytes 9220
  154.9 2.5 %copy-start.6 = (f32[1,3,128,2,128]{4,2,1,3,0:T(8,128)S(1)}, f32[1,3,128,2,128]{4,2,1,3,0:T(8,128)}, u32[]{:S(2)}) copy-start(f32[1,3,128,2,128]{4,2,1,3,0:T(8,128)} %copy.127) | copy-start | bytes 1179652
  154.9 2.5 %copy-start.7 = (f32[96,4,2,128]{3,1,0,2:T(4,128)S(1)}, f32[96,4,2,128]{3,1,0,2:T(4,128)}, u32[]{:S(2)}) copy-start(f32[96,4,2,128]{3,1,0,2:T(4,128)} %copy.130) | copy-start | bytes 1179652
  (10 other events, 9.0 us)
where the time goes:
time: 179 us; the launch traced here: 178 us
  waiting for transfers between devices  79.4 us (44%)
  local copies, waits for them, and re-layouts  37.9 us (21%)
  starting transfers between devices  18 us (10%)
  blocking collectives  17 us (9%)
  matrix products  14.4 us (8%)
  other arithmetic  9.77 us (5%)
    ppermute x3, waiting for transfers between devices, from_behind(): lax.ppermute(value, axis, [(source, source + steps) for source in range(i...  65.7 us
    all_to_all x1, blocking collectives, sent_to_all(): lax.all_to_all(jnp.broadcast_to(shard[None], (length, *shard.shape)), axi...  17 us
    unnamed x66, local copies, waits for them, and re-layouts  15.5 us
    all_to_all x1, waiting for transfers between devices, sent_to_all(): lax.all_to_all(jnp.broadcast_to(shard[None], (length, *shard.shape)), axi...  13.7 us
    ppermute x3, starting transfers between devices, from_behind(): lax.ppermute(value, axis, [(source, source + steps) for source in range(i...  8.99 us
    dot_general x3, matrix products, local_branch(): jnp.einsum('rnqhd,rnkhd->rnhqk', query_blocks, key_blocks, preferred_elem...  5.38 us
    all_to_all x1, starting transfers between devices, sent_to_all(): lax.all_to_all(jnp.broadcast_to(shard[None], (length, *shard.shape)), axi...  4.71 us
    all_to_all x1, starting transfers between devices, local(): lax.all_to_all(w_out, 'tp', split_axis=1, concat_axis=0, tiled=True)  4.34 us
  transfers between devices with their start and end apart: 5, of which 4 were waited for; matrix products, arithmetic and copies ran while one was open for 30% of the time, Pallas kernels for 0%

commit v1 on v0

v1 whole, which is shorter than its diff:
```python
import functools

import jax
import jax.numpy as jnp
import numpy as np
from jax import lax
from jax.experimental import pallas as pl
from jax.experimental.pallas import tpu as pltpu
from jax.sharding import PartitionSpec as P

KEYS_BEHIND = 128
MIDDLE = 4
WIDEST = 16
EPSILON = 1e-06
ROTARY_BASE = 500000.0
NEG = -1e30

NC = MIDDLE
NI = WIDEST // MIDDLE
BF = jnp.bfloat16
F32 = jnp.float32
MESH = pl.DeviceIdType.MESH


def dot(a, b):
    return jnp.dot(a, b, preferred_element_type=F32)


def dot_nt(a, b):
    return lax.dot_general(a, b, (((1,), (1,)), ((), ())), preferred_element_type=F32)


def iota(shape, dim):
    return lax.broadcasted_iota(jnp.int32, shape, dim)


def kernel(
    n_tp, n_sp,
    hid_h, ngain, wq_h, wk_h, wv_h, qg_ref, kg_ref, wo_h, tabc_h, tabs_h, basec, bases,
    out_ref, log_ref,
    hid_v, hx, w_v, tabc, tabs, wcol, sbuf, fbuf, qb, kv, bias1, bias1e, bias4, bias16,
    o1, o4, o16, e1, e4, e16, attb, attl, attx, ag, lt, mm, macc,
    lsem, xs_own, xr_own, xs_fwd, xr_fwd, ds_q, dr_q, zs, zr, ws, wr, wds, wdr,
    ds_a, dr_a, ds_l, dr_l, as_own, ar_own, as_fwd, ar_fwd,
):
    tok, width = hid_v.shape
    rows = tok // NC
    half = rows // 2
    nj = tok // WIDEST
    cj = 2 * nj
    hd = KEYS_BEHIND
    depth = n_tp * width
    wo_rows = wo_h.shape[0]
    own0 = kv.shape[2] - cj
    n_near = own0 - cj
    n_far = n_near - cj
    last = n_far

    me = lax.axis_index("tp")
    sp = lax.axis_index("sp")
    core = lax.rem(sp, 2)
    other = 1 - core
    z = lax.div(sp, 2)
    lf = lax.rem(me + n_tp - 1, n_tp)
    rt = lax.rem(me + 1, n_tp)
    op = lax.rem(me + 2, n_tp)
    partner = sp + 1 - 2 * core
    up = lax.rem(sp + 2, n_sp)
    down = lax.rem(sp + n_sp - 2, n_sp)
    to_rt, to_lf, to_op = {"tp": rt}, {"tp": lf}, {"tp": op}
    to_partner, to_up, to_down = {"sp": partner}, {"sp": up}, {"sp": down}
    joff = pl.multiple_of(core * nj, 8)
    poff = pl.multiple_of(other * nj, 8)

    pending = []

    def send(src, dst, ssem, rsem, dev):
        copy = pltpu.make_async_remote_copy(
            src_ref=src, dst_ref=dst, send_sem=ssem, recv_sem=rsem, device_id=dev, device_id_type=MESH
        )
        copy.start()
        pending.append(copy)
        return copy

    def load(src, dst, k):
        copy = pltpu.make_async_copy(src, dst, lsem.at[k])
        copy.start()
        return copy

    c_hid = load(hid_h, hid_v, 0)
    for stage, (lo, hi) in enumerate(((n_near, own0), (n_far, n_near), (0, n_far))):
        @pl.when(z <= stage)
        def _():
            kv[:, :, lo:hi, :] = jnp.zeros((2, WIDEST, hi - lo, hd), BF)
    barrier = pltpu.get_barrier_semaphore()
    for dev in (to_rt, to_lf, to_op, to_partner):
        pl.semaphore_signal(barrier, inc=1, device_id=dev, device_id_type=MESH)
    has_up, has_down = z < n_sp // 2 - 1, z > 0

    @pl.when(has_up)
    def _():
        pl.semaphore_signal(barrier, inc=1, device_id=to_up, device_id_type=MESH)

    @pl.when(has_down)
    def _():
        pl.semaphore_signal(barrier, inc=1, device_id=to_down, device_id_type=MESH)

    own_col = pl.ds(pl.multiple_of(core * hd, hd), hd)
    oth_col = pl.ds(pl.multiple_of(other * hd, hd), hd)
    c_w = []
    for n, w in enumerate((wq_h, wk_h, wv_h)):
        c_w.append(load(w.at[:, own_col], w_v.at[:, pl.ds(n * hd, hd)], 1 + 2 * n))
        c_w.append(load(w.at[:, oth_col], w_v.at[:, pl.ds((3 + n) * hd, hd)], 2 + 2 * n))
    c_t = [load(tabc_h, tabc, 7), load(tabs_h, tabs, 8)]
    my_cols = pl.ds(pl.multiple_of(me * width, width), width)
    my_rows = pl.ds(pl.multiple_of(me * wo_rows, wo_rows), wo_rows)
    c_wo = load(wo_h.at[:, my_cols], wcol.at[my_rows, :], 9)

    prow = iota((tok, tok), 0)
    pcol = iota((tok, tok), 1)
    place = (pcol & (NC - 1)) * rows + ((pcol >> 2) & (NI - 1)) * nj + (pcol >> 4)
    perm = jnp.where(prow == place, 1.0, 0.0).astype(BF)
    c_hid.wait()
    mine = dot(perm, hid_v[...]).astype(BF)
    hx[me] = mine
    pl.semaphore_wait(barrier, 4 + has_up.astype(jnp.int32) + has_down.astype(jnp.int32))

    def x_own(c):
        part = hx.at[me, pl.ds(c * rows, rows), :]
        return (
            send(part, part, xs_own.at[c, 0], xr_own.at[c, 0], to_rt),
            send(part, part, xs_own.at[c, 1], xr_own.at[c, 1], to_lf),
        )

    x_sent = {0: x_own(0), 1: x_own(1)}

    for c in c_t:
        c.wait()
    bc, bs = basec[pl.ds(sp, 1), :], bases[pl.ds(sp, 1), :]
    oc, os_ = tabc[...], tabs[...]
    sign = jnp.where(iota((1, hd), 1) < hd // 2, -1.0, 1.0)
    tabc[...] = bc * oc - bs * os_
    tabs[...] = (bs * oc + bc * os_) * sign

    first_j = own0 - cj * z
    jq = iota((cj, own0 + cj), 0)
    jk = iota((cj, own0 + cj), 1)
    ok = (jk >= jq) & (jk <= jq + KEYS_BEHIND) & (jk >= first_j)
    bias16[...] = jnp.where(ok, 0.0, NEG)
    w4 = bias4.shape[1] // NI
    row = iota(bias4.shape, 0)
    col = iota(bias4.shape, 1)
    iq = (row * (65536 // cj + 1)) >> 16
    ik = (col * (65536 // w4 + 1)) >> 16
    j4 = own0 + cj - w4
    jk = j4 + col - ik * w4
    dist = NI * (own0 + (row - iq * cj) - jk) + iq - ik
    ok = (dist >= 0) & (dist <= KEYS_BEHIND) & (jk >= first_j)
    bias4[...] = jnp.where(ok, 0.0, NEG)
    row = iota(bias1.shape, 0)
    col = iota(bias1.shape, 1)
    uq = row >> 4
    uk = col >> 5
    rq = (uq >> 2) + NC * (uq & (NI - 1))
    rk = (uk >> 2) + NC * (uk & (NI - 1))
    dist = WIDEST * ((row & 15) + 16 - (col & 31)) + rq - rk
    ok = (dist >= 0) & (dist <= KEYS_BEHIND)
    bias1[...] = jnp.where(ok, 0.0, NEG)
    bias1e[...] = jnp.where(ok & ((col & 31) + own0 - 16 >= first_j), 0.0, NEG)

    def partial(c, s, acc, sq):
        h = hx[s, c * rows : (c + 1) * rows, :].astype(F32)
        sc = (h * ngain[s]).astype(BF)
        sq = sq + jnp.sum(h * h, axis=1, keepdims=True)
        acc = acc + dot(sc, w_v[pl.ds(pl.multiple_of(s * width, width), width), :])
        return acc, sq

    def head_rows(x, gain, cos, sin):
        x = x * lax.rsqrt(jnp.mean(x * x, axis=1, keepdims=True) + EPSILON) * gain
        return x * cos + pltpu.roll(x, hd // 2, 1) * sin

    def epilogue(c, acc, sq):
        rs = lax.rsqrt(sq / depth + EPSILON)
        cos = tabc[c * rows : (c + 1) * rows, :]
        sin = tabs[c * rows : (c + 1) * rows, :]
        parts = []
        for side, hidx in ((1, other), (0, core)):
            x = [acc[:, (3 * side + n) * hd : (3 * side + n + 1) * hd] * rs for n in range(3)]
            q = head_rows(x[0], qg_ref[hidx], cos, sin)
            k = head_rows(x[1], kg_ref[hidx], cos, sin)
            parts = [v.reshape(NI, nj, hd) for v in (q, k, x[2])]
            for n in range(3):
                if side == 1:
                    sbuf[n, c * NI : (c + 1) * NI, :, :] = parts[n]
                else:
                    fbuf[n, c * NI : (c + 1) * NI, pl.ds(joff, nj), :] = parts[n]
        return send(
            sbuf.at[:, pl.ds(c * NI, NI), :, :],
            fbuf.at[:, pl.ds(c * NI, NI), pl.ds(joff, nj), :],
            ds_q.at[c], dr_q.at[c], to_partner,
        )

    z_copies = {}
    for stage, (start, count, to) in enumerate(
        ((own0, cj, n_near), (n_near, cj, n_far), (n_far + cj - last, last, 0))
    ):
        for c in range(NC):
            u = pl.ds(c * NI, NI)
            z_copies[stage, c] = pltpu.make_async_remote_copy(
                src_ref=kv.at[:, u, pl.ds(start, count), :], dst_ref=kv.at[:, u, pl.ds(to, count), :],
                send_sem=zs.at[stage, c], recv_sem=zr.at[stage, c], device_id=to_up, device_id_type=MESH,
            )

    def z_send(stage, c):
        @pl.when((z >= stage) & has_up)
        def _():
            z_copies[stage, c].start()

    def z_wait(stage, c):
        @pl.when(z > stage)
        def _():
            z_copies[stage, c].wait_recv()

    def z_pass(stage, c):
        z_wait(stage, c)
        z_send(stage + 1, c)

    def own_pair(c, copy):
        copy.wait_recv()
        u = slice(c * NI, (c + 1) * NI)
        kv[0, u, own0:, :] = fbuf[1, u].astype(BF)
        kv[1, u, own0:, :] = fbuf[2, u].astype(BF)
        z_send(0, c)
        qb[u] = fbuf[0, u].astype(BF)

    for c in c_w:
        c.wait()
    for c in range(NC):
        right, left = x_sent[c]
        right.wait_recv()
        h0 = hx.at[lf, pl.ds(c * rows, half), :]
        f0 = send(h0, h0, xs_fwd.at[c, 0], xr_fwd.at[c, 0], to_rt)
        left.wait_recv()
        h1 = hx.at[rt, pl.ds(c * rows + half, half), :]
        f1 = send(h1, h1, xs_fwd.at[c, 1], xr_fwd.at[c, 1], to_lf)
        if c + 2 < NC:
            x_sent[c + 2] = x_own(c + 2)
        acc = jnp.zeros((rows, 6 * hd), F32)
        sq = jnp.zeros((rows, 1), F32)
        for s in (me, lf, rt):
            acc, sq = partial(c, s, acc, sq)
        if c >= 2:
            z_pass(0, c - 2)
        f0.wait_recv()
        f1.wait_recv()
        acc, sq = partial(c, op, acc, sq)
        own_pair(c, epilogue(c, acc, sq))

    wh = wo_rows // 2
    w_sent = []
    for n, dst in ((1, rt), (3, lf), (2, op)):
        src = wo_h.at[pl.ds(pl.multiple_of(core * wh, wh), wh), pl.ds(pl.multiple_of(dst * width, width), width)]
        to = wcol.at[pl.ds(pl.multiple_of(me * wo_rows + core * wh, wh), wh), :]
        w_sent.append(send(src, to, ws.at[n - 1], wr.at[n - 1], {"tp": dst}))

    def w_pass():
        fwd = []
        for k, (n, src) in enumerate(((1, lf), (3, rt), (2, op))):
            w_sent[k].wait_recv()
            part = wcol.at[pl.ds(pl.multiple_of(src * wo_rows + core * wh, wh), wh), :]
            fwd.append(send(part, part, wds.at[n - 1], wdr.at[n - 1], to_partner))
        return fwd

    def softmax(s, bias):
        s = s * (hd ** -0.5) + bias
        m = jnp.max(s, axis=1, keepdims=True)
        w = jnp.exp(s - m)
        l = jnp.sum(w, axis=1, keepdims=True)
        return w.astype(BF), m, l

    def wide(x):
        return jnp.broadcast_to(x, (x.shape[0], hd))

    def branch1(b):
        q = qb[:, 16 * b : 16 * b + 16, :].reshape(WIDEST * 16, hd)
        lo = own0 - 16 + 16 * b
        k = kv[0, :, lo : lo + 32, :].reshape(WIDEST * 32, hd)
        v = kv[1, :, lo : lo + 32, :].reshape(WIDEST * 32, hd)
        w, m, l = softmax(dot_nt(q, k), (bias1e if b == 0 else bias1)[...])
        o1[:, 16 * b : 16 * b + 16, :] = (dot(w, v) / l).reshape(WIDEST, 16, hd)
        e1[:, 16 * b : 16 * b + 16, :] = wide(m + jnp.log(l)).reshape(WIDEST, 16, hd)

    def branch4(c):
        u = slice(c * NI, (c + 1) * NI)
        q = qb[u].reshape(NI * cj, hd)
        k = kv[0, u, j4:, :].reshape(NI * w4, hd)
        v = kv[1, u, j4:, :].reshape(NI * w4, hd)
        w, m, l = softmax(dot_nt(q, k), bias4[...])
        o4[u] = (dot(w, v) / l).reshape(NI, cj, hd)
        e4[u] = wide(m + jnp.log(l)).reshape(NI, cj, hd)

    def branch16(c):
        for u in range(c * NI, (c + 1) * NI):
            w, m, l = softmax(dot_nt(qb[u], kv[0, u]), bias16[...])
            o16[u] = dot(w, kv[1, u]) / l
            e16[u] = wide(m + jnp.log(l))

    def finish(c):
        u = slice(c * NI, (c + 1) * NI)
        a, b, d = e1[u], e4[u], e16[u]
        top = jnp.maximum(jnp.maximum(a, b), d)
        total = top + jnp.log(jnp.exp(a - top) + jnp.exp(b - top) + jnp.exp(d - top))
        att = jnp.exp(a - total) * o1[u] + jnp.exp(b - total) * o4[u] + jnp.exp(d - total) * o16[u]
        attb[c] = att
        attl[c] = total
        attx[c] = attb[c, :, pl.ds(poff, nj), :].reshape(rows, hd).astype(BF)
        ag[me, c, core] = attb[c, :, pl.ds(joff, nj), :].reshape(rows, hd).astype(BF)
        lt[core, c] = attl[c, :, pl.ds(joff, nj), :]
        return (
            send(attx.at[c], ag.at[me, c, core], ds_a.at[c], dr_a.at[c], to_partner),
            send(attl.at[c, :, pl.ds(poff, nj), :], lt.at[core, c], ds_l.at[c], dr_l.at[c], to_partner),
        )

    def a_own(c, copies):
        copies[0].wait_recv()
        part = ag.at[me, c]
        return (
            send(part, part, as_own.at[c, 0], ar_own.at[c, 0], to_rt),
            send(part, part, as_own.at[c, 1], ar_own.at[c, 1], to_lf),
        )

    def a_fwd(c, copies):
        copies[0].wait_recv()
        p0 = ag.at[lf, c, 0]
        f0 = send(p0, p0, as_fwd.at[c, 0], ar_fwd.at[c, 0], to_rt)
        copies[1].wait_recv()
        p1 = ag.at[rt, c, 1]
        f1 = send(p1, p1, as_fwd.at[c, 1], ar_fwd.at[c, 1], to_lf)
        return f0, f1

    def a_mix(c, copies):
        for f in copies:
            f.wait_recv()
        lhs = jnp.concatenate([ag[s, c, h] for s in range(n_tp) for h in range(2)], axis=1)
        mm[c * rows : (c + 1) * rows, :] = dot(lhs, wcol[...]).astype(BF)

    t0 = iota((tok, rows), 0)
    q0 = iota((tok, rows), 1)

    def back(c):
        there = ((t0 & (NC - 1)) == c) & (q0 == ((t0 >> 2) & (NI - 1)) * nj + (t0 >> 4))
        return jnp.where(there, 1.0, 0.0).astype(BF)

    z_pass(1, 0)
    z_pass(0, 2)
    branch4(0)
    z_pass(1, 1)
    branch4(1)
    z_pass(0, 3)
    branch4(2)
    z_wait(2, 0)
    branch16(0)
    z_pass(1, 2)
    branch1(0)
    branch1(1)
    branch1(2)
    branch4(3)
    d0 = finish(0)
    z_wait(2, 1)
    branch16(1)
    z_pass(1, 3)
    d1 = finish(1)
    w_fwd = w_pass()
    a0 = a_own(0, d0)
    a1 = a_own(1, d1)
    f_0 = a_fwd(0, a0)
    c_wo.wait()
    for f in w_fwd:
        f.wait_recv()
    a_mix(0, f_0)
    z_wait(2, 2)
    branch16(2)
    d2 = finish(2)
    f_1 = a_fwd(1, a1)
    a_mix(1, f_1)
    a2 = a_own(2, d2)
    z_wait(2, 3)
    branch16(3)
    d3 = finish(3)
    f_2 = a_fwd(2, a2)
    a3 = a_own(3, d3)
    a_mix(2, f_2)
    macc[...] = sum(dot(back(c), mm[c * rows : (c + 1) * rows, :]) for c in range(3))
    for d in (d0, d1, d2, d3):
        d[1].wait_recv()
    lane = iota((1, hd), 1)
    acc = jnp.zeros((tok, hd), F32)
    for c in range(NC):
        x = jnp.where(lane == 0, lt[0, c].reshape(rows, hd), lt[1, c].reshape(rows, hd))
        hi = x.astype(BF)
        rest = x - hi.astype(F32)
        mid = rest.astype(BF)
        low = (rest - mid.astype(F32)).astype(BF)
        p = back(c)
        acc = acc + (dot(p, hi) + dot(p, mid) + dot(p, low))
    log_ref[...] = acc[:, :2]
    f_3 = a_fwd(3, a3)
    a_mix(3, f_3)
    out_ref[...] = (macc[...] + dot(back(3), mm[3 * rows :, :])).astype(BF)
    for copy in pending:
        copy.wait_send()
    for stage in range(3):
        @pl.when((z >= stage) & has_up)
        def _():
            for c in range(NC):
                z_copies[stage, c].wait_send()


def tables(tok, n_sp, hd):
    inv = ROTARY_BASE ** (-np.arange(0, hd, 2, dtype=np.float64) / hd)
    inv = np.concatenate([inv, inv]).astype(np.float32).astype(np.float64)
    nj = tok // WIDEST
    c, i, j = np.meshgrid(np.arange(NC), np.arange(NI), np.arange(nj), indexing="ij")
    off = (WIDEST * j + c + NC * i).reshape(-1).astype(np.float64)
    base = np.arange(n_sp, dtype=np.float64) * tok
    out = []
    for p in (off, base):
        a = p[:, None] * inv[None, :]
        out += [np.cos(a).astype(np.float32), np.sin(a).astype(np.float32)]
    return out


def local(n_tp, n_sp, hidden, norm_gain, w_query, w_key, w_value, query_gain, key_gain, w_out):
    tok, width = hidden.shape
    heads, hd = query_gain.shape
    rows = tok // NC
    nj = tok // WIDEST
    cj = 2 * nj
    keys = cj + KEYS_BEHIND
    w4 = cj + KEYS_BEHIND // NI
    tabc, tabs, basec, bases = tables(tok, n_sp, hd)
    dma = pltpu.SemaphoreType.DMA
    vm = pltpu.VMEM
    scratch = [
        vm((tok, width), BF),
        vm((n_tp, tok, width), BF),
        vm((n_tp * width, 6 * hd), BF),
        vm((tok, hd), F32), vm((tok, hd), F32),
        vm((n_tp * heads * hd, width), BF),
        vm((3, WIDEST, nj, hd), F32),
        vm((3, WIDEST, cj, hd), F32),
        vm((WIDEST, cj, hd), BF),
        vm((2, WIDEST, keys, hd), BF),
        vm((WIDEST * 16, WIDEST * 32), F32), vm((WIDEST * 16, WIDEST * 32), F32),
        vm((NI * cj, NI * w4), F32),
        vm((cj, keys), F32),
        vm((WIDEST, cj, hd), F32), vm((WIDEST, cj, hd), F32), vm((WIDEST, cj, hd), F32),
        vm((WIDEST, cj, hd), F32), vm((WIDEST, cj, hd), F32), vm((WIDEST, cj, hd), F32),
        vm((NC, NI, cj, hd), F32),
        vm((NC, NI, cj, hd), F32),
        vm((NC, rows, hd), BF),
        vm((n_tp, NC, 2, rows, hd), BF),
        vm((2, NC, NI, nj, hd), F32),
        vm((tok, width), BF),
        vm((tok, width), F32),
        dma((10,)),
        dma((NC, 2)), dma((NC, 2)), dma((NC, 2)), dma((NC, 2)),
        dma((NC,)), dma((NC,)),
        dma((3, NC)), dma((3, NC)),
        dma((3,)), dma((3,)), dma((3,)), dma((3,)),
        dma((NC,)), dma((NC,)), dma((NC,)), dma((NC,)),
        dma((NC, 2)), dma((NC, 2)), dma((NC, 2)), dma((NC, 2)),
    ]
    hbm = pl.BlockSpec(memory_space=pl.ANY)
    vmem = pl.BlockSpec(memory_space=pltpu.VMEM)
    return pl.pallas_call(
        functools.partial(kernel, n_tp, n_sp),
        out_shape=(
            jax.ShapeDtypeStruct((tok, width), BF),
            jax.ShapeDtypeStruct((tok, heads), F32),
        ),
        in_specs=[hbm, vmem, hbm, hbm, hbm, vmem, vmem, hbm, hbm, hbm, vmem, vmem],
        out_specs=(vmem, vmem),
        scratch_shapes=scratch,
        compiler_params=pltpu.CompilerParams(
            collective_id=0, has_side_effects=True, vmem_limit_bytes=62 * 1024 * 1024
        ),
    )(
        hidden, norm_gain.astype(F32).reshape(n_tp, 1, width), w_query, w_key, w_value,
        query_gain.reshape(heads, 1, hd), key_gain.reshape(heads, 1, hd), w_out,
        jnp.asarray(tabc), jnp.asarray(tabs), jnp.asarray(basec), jnp.asarray(bases),
    )


def solution(mesh):
    placed = (
        P(("grp", "sp"), "tp"),
        P(),
        P(None, "tp"),
        P(None, "tp"),
        P(None, "tp"),
        P("tp", None),
        P("tp", None),
        P("tp", None),
    )
    return jax.shard_map(
        functools.partial(local, mesh.shape["tp"], mesh.shape["sp"]),
        mesh=mesh,
        in_specs=placed,
        out_specs=(P(("grp", "sp"), "tp"), P(("grp", "sp"), "tp")),
        check_vma=False,
    )
```

time: 179 us -> 107 us (0.60)
  the two profiles are of different devices: /device:TPU:96 before, /device:TPU:34 now
where the time goes in v1:
time: 107 us
  Pallas kernels  102 us (95%)
  local copies, waits for them, and re-layouts  3.38 us (3%)
  other arithmetic  1.29 us (1%)
    pallas_call x1, Pallas kernels, local(): pl.pallas_call(functools.partial(kernel, n_tp, n_sp), out_shape=(jax.Shap...  102 us

profile of v1, /device:TPU:34, one launch (start us, length us, event | category | flops | bytes accessed | tf_op | source)
XLA Modules:
  0.0 106.9 jit_solution(1426111243103361927)
XLA Ops:
  0.6 1.3 %reshape.19 = f32[2048]{0:T(1024)} convert(bf16[2048]{0:T(1024)(128)(2,1)} %param.13) | non-fusion elementwise | flops 2048 | bytes 12288 | tf_op jit(solution)/shard_map/reshape | solution.py:489
  1.9 101.6 %shard_map.131 = (bf16[384,512]{1,0:T(8,128)(2,1)}, f32[384,2]{1,0:T(8,128)}) custom-call(bf16[384,512]{1,0:T(8,128)(2,1)} %hid_h.1, f32[4,1,512]{2,1,0:T(1,128)} %bitcast.3, bf16[2048,256]{1,0:T(8,128)(2,1)} %wq_h.1, bf16[2048,256]{1,0:T(8,128)(2,1)} %wk_h.1, bf16[2048,256]{1,0:T(8,128)(2,1)} %wv_h.1, f32[2,1,128]{2,1,0:T(1,128)} %bitcast.4, ...), custom_call_target="tpu_custom_call" | custom-call | tf_op jit(solution)/shard_map/pallas_call | solution.py:476
  103.5 1.6 %copy.14 = f32[384,2]{0,1:T(2,128)} copy(f32[384,2]{1,0:T(8,128)} %get-tuple-element.3) | data formatting | bytes 6144 | tf_op jit(solution)/shard_map/pallas_call | solution.py:476
  105.1 1.8 %copy.16 = bf16[384,512]{1,0:T(8,128)(2,1)} copy(bf16[384,512]{1,0:T(8,128)(2,1)} %get-tuple-element.6) | data formatting | bytes 786432

commit v2 on v1

--- a/solution.py
+++ b/solution.py
@@ -30,15 +30,19 @@
     return lax.dot_general(a, b, (((1,), (1,)), ((), ())), preferred_element_type=F32)
 
 
+def dot_tn(a, b):
+    return lax.dot_general(a, b, (((0,), (0,)), ((), ())), preferred_element_type=F32)
+
+
 def iota(shape, dim):
     return lax.broadcasted_iota(jnp.int32, shape, dim)
 
 
 def kernel(
     n_tp, n_sp,
-    hid_h, ngain, wq_h, wk_h, wv_h, qg_ref, kg_ref, wo_h, tabc_h, tabs_h, basec, bases,
+    hid_h, ng_h, wq_h, wk_h, wv_h, qg_h, kg_h, wo_h, tabc_h, tabs_h, basec_h, bases_h,
     out_ref, log_ref,
-    hid_v, hx, w_v, tabc, tabs, wcol, sbuf, fbuf, qb, kv, bias1, bias1e, bias4, bias16,
+    hid_v, ng_v, ngain, qg_ref, kg_ref, basec, bases, hx, w_v, tabc, tabs, wcol, sbuf, fbuf, qb, kv, bias1, bias1e, bias4, bias16,
     o1, o4, o16, e1, e4, e16, attb, attl, attx, ag, lt, mm, macc,
     lsem, xs_own, xr_own, xs_fwd, xr_fwd, ds_q, dr_q, zs, zr, ws, wr, wds, wdr,
     ds_a, dr_a, ds_l, dr_l, as_own, ar_own, as_fwd, ar_fwd,
@@ -112,6 +116,10 @@
         c_w.append(load(w.at[:, own_col], w_v.at[:, pl.ds(n * hd, hd)], 1 + 2 * n))
         c_w.append(load(w.at[:, oth_col], w_v.at[:, pl.ds((3 + n) * hd, hd)], 2 + 2 * n))
     c_t = [load(tabc_h, tabc, 7), load(tabs_h, tabs, 8)]
+    for n, (src, dst) in enumerate(
+        ((ng_h, ng_v), (qg_h, qg_ref), (kg_h, kg_ref), (basec_h.at[pl.ds(sp, 1)], basec), (bases_h.at[pl.ds(sp, 1)], bases))
+    ):
+        c_t.append(load(src, dst, 10 + n))
     my_cols = pl.ds(pl.multiple_of(me * width, width), width)
     my_rows = pl.ds(pl.multiple_of(me * wo_rows, wo_rows), wo_rows)
     c_wo = load(wo_h.at[:, my_cols], wcol.at[my_rows, :], 9)
@@ -120,10 +128,12 @@
     pcol = iota((tok, tok), 1)
     place = (pcol & (NC - 1)) * rows + ((pcol >> 2) & (NI - 1)) * nj + (pcol >> 4)
     perm = jnp.where(prow == place, 1.0, 0.0).astype(BF)
-    c_hid.wait()
+    with jax.named_scope("hid_wait"):
+        c_hid.wait()
     mine = dot(perm, hid_v[...]).astype(BF)
     hx[me] = mine
-    pl.semaphore_wait(barrier, 4 + has_up.astype(jnp.int32) + has_down.astype(jnp.int32))
+    with jax.named_scope("barrier_wait"):
+        pl.semaphore_wait(barrier, 4 + has_up.astype(jnp.int32) + has_down.astype(jnp.int32))
 
     def x_own(c):
         part = hx.at[me, pl.ds(c * rows, rows), :]
@@ -136,12 +146,17 @@
 
     for c in c_t:
         c.wait()
-    bc, bs = basec[pl.ds(sp, 1), :], bases[pl.ds(sp, 1), :]
+    bc, bs = basec[0], bases[0]
     oc, os_ = tabc[...], tabs[...]
     sign = jnp.where(iota((1, hd), 1) < hd // 2, -1.0, 1.0)
     tabc[...] = bc * oc - bs * os_
     tabs[...] = (bs * oc + bc * os_) * sign
 
+    gains = ng_v[...].astype(F32)
+    for s in range(n_tp):
+        for k in range(width // hd):
+            r = s * (width // hd) + k
+            ngain[s, :, k * hd : (k + 1) * hd] = gains[r : r + 1, :]
     first_j = own0 - cj * z
     jq = iota((cj, own0 + cj), 0)
     jk = iota((cj, own0 + cj), 1)
@@ -168,6 +183,7 @@
     bias1[...] = jnp.where(ok, 0.0, NEG)
     bias1e[...] = jnp.where(ok & ((col & 31) + own0 - 16 >= first_j), 0.0, NEG)
 
+    @jax.named_scope('partial')
     def partial(c, s, acc, sq):
         h = hx[s, c * rows : (c + 1) * rows, :].astype(F32)
         sc = (h * ngain[s]).astype(BF)
@@ -179,6 +195,7 @@
         x = x * lax.rsqrt(jnp.mean(x * x, axis=1, keepdims=True) + EPSILON) * gain
         return x * cos + pltpu.roll(x, hd // 2, 1) * sin
 
+    @jax.named_scope('epilogue')
     def epilogue(c, acc, sq):
         rs = lax.rsqrt(sq / depth + EPSILON)
         cos = tabc[c * rows : (c + 1) * rows, :]
@@ -186,8 +203,8 @@
         parts = []
         for side, hidx in ((1, other), (0, core)):
             x = [acc[:, (3 * side + n) * hd : (3 * side + n + 1) * hd] * rs for n in range(3)]
-            q = head_rows(x[0], qg_ref[hidx], cos, sin)
-            k = head_rows(x[1], kg_ref[hidx], cos, sin)
+            q = head_rows(x[0], qg_ref[pl.ds(hidx, 1), :], cos, sin)
+            k = head_rows(x[1], kg_ref[pl.ds(hidx, 1), :], cos, sin)
             parts = [v.reshape(NI, nj, hd) for v in (q, k, x[2])]
             for n in range(3):
                 if side == 1:
@@ -216,17 +233,21 @@
         def _():
             z_copies[stage, c].start()
 
+    @jax.named_scope('z_wait')
     def z_wait(stage, c):
         @pl.when(z > stage)
         def _():
             z_copies[stage, c].wait_recv()
 
+    @jax.named_scope('z_pass')
     def z_pass(stage, c):
         z_wait(stage, c)
         z_send(stage + 1, c)
 
+    @jax.named_scope('own_pair')
     def own_pair(c, copy):
-        copy.wait_recv()
+        with jax.named_scope("pair_wait"):
+            copy.wait_recv()
         u = slice(c * NI, (c + 1) * NI)
         kv[0, u, own0:, :] = fbuf[1, u].astype(BF)
         kv[1, u, own0:, :] = fbuf[2, u].astype(BF)
@@ -235,12 +256,14 @@
 
     for c in c_w:
         c.wait()
-    for c in range(NC):
+    def x_step(c):
         right, left = x_sent[c]
-        right.wait_recv()
+        with jax.named_scope("x_wait"):
+            right.wait_recv()
         h0 = hx.at[lf, pl.ds(c * rows, half), :]
         f0 = send(h0, h0, xs_fwd.at[c, 0], xr_fwd.at[c, 0], to_rt)
-        left.wait_recv()
+        with jax.named_scope("x_wait"):
+            left.wait_recv()
         h1 = hx.at[rt, pl.ds(c * rows + half, half), :]
         f1 = send(h1, h1, xs_fwd.at[c, 1], xr_fwd.at[c, 1], to_lf)
         if c + 2 < NC:
@@ -249,20 +272,36 @@
         sq = jnp.zeros((rows, 1), F32)
         for s in (me, lf, rt):
             acc, sq = partial(c, s, acc, sq)
+        return acc, sq, f0, f1
+
+    def x_end(c, state):
+        acc, sq, f0, f1 = state
+        with jax.named_scope("xf_wait"):
+            f0.wait_recv()
+            f1.wait_recv()
+        acc, sq = partial(c, op, acc, sq)
+        return epilogue(c, acc, sq)
+
+    state, pairs = {}, {}
+    for c in range(NC):
+        state[c] = x_step(c)
         if c >= 2:
-            z_pass(0, c - 2)
-        f0.wait_recv()
-        f1.wait_recv()
-        acc, sq = partial(c, op, acc, sq)
-        own_pair(c, epilogue(c, acc, sq))
+            own_pair(c - 2, pairs[c - 2])
+        if c >= 3:
+            z_pass(0, c - 3)
+        if c >= 1:
+            pairs[c - 1] = x_end(c - 1, state[c - 1])
 
     wh = wo_rows // 2
     w_sent = []
-    for n, dst in ((1, rt), (3, lf), (2, op)):
-        src = wo_h.at[pl.ds(pl.multiple_of(core * wh, wh), wh), pl.ds(pl.multiple_of(dst * width, width), width)]
-        to = wcol.at[pl.ds(pl.multiple_of(me * wo_rows + core * wh, wh), wh), :]
-        w_sent.append(send(src, to, ws.at[n - 1], wr.at[n - 1], {"tp": dst}))
-
+
+    def w_start():
+        for n, dst in ((1, rt), (3, lf), (2, op)):
+            src = wo_h.at[pl.ds(pl.multiple_of(core * wh, wh), wh), pl.ds(pl.multiple_of(dst * width, width), width)]
+            to = wcol.at[pl.ds(pl.multiple_of(me * wo_rows + core * wh, wh), wh), :]
+            w_sent.append(send(src, to, ws.at[n - 1], wr.at[n - 1], {"tp": dst}))
+
+    @jax.named_scope('w_pass')
     def w_pass():
         fwd = []
         for k, (n, src) in enumerate(((1, lf), (3, rt), (2, op))):
@@ -281,6 +320,7 @@
     def wide(x):
         return jnp.broadcast_to(x, (x.shape[0], hd))
 
+    @jax.named_scope('branch1')
     def branch1(b):
         q = qb[:, 16 * b : 16 * b + 16, :].reshape(WIDEST * 16, hd)
         lo = own0 - 16 + 16 * b
@@ -290,6 +330,7 @@
         o1[:, 16 * b : 16 * b + 16, :] = (dot(w, v) / l).reshape(WIDEST, 16, hd)
         e1[:, 16 * b : 16 * b + 16, :] = wide(m + jnp.log(l)).reshape(WIDEST, 16, hd)
 
+    @jax.named_scope('branch4')
     def branch4(c):
         u = slice(c * NI, (c + 1) * NI)
         q = qb[u].reshape(NI * cj, hd)
@@ -299,12 +340,17 @@
         o4[u] = (dot(w, v) / l).reshape(NI, cj, hd)
         e4[u] = wide(m + jnp.log(l)).reshape(NI, cj, hd)
 
+    @jax.named_scope('branch16')
     def branch16(c):
-        for u in range(c * NI, (c + 1) * NI):
-            w, m, l = softmax(dot_nt(qb[u], kv[0, u]), bias16[...])
-            o16[u] = dot(w, kv[1, u]) / l
-            e16[u] = wide(m + jnp.log(l))
-
+        us = range(c * NI, (c + 1) * NI)
+        s = jnp.concatenate([dot_nt(qb[u], kv[0, u]) for u in us], axis=0)
+        w, m, l = softmax(s, jnp.concatenate([bias16[...]] * NI, axis=0))
+        e16[c * NI : (c + 1) * NI] = wide(m + jnp.log(l)).reshape(NI, cj, hd)
+        for n, u in enumerate(us):
+            part = slice(n * cj, (n + 1) * cj)
+            o16[u] = dot(w[part], kv[1, u]) / l[part]
+
+    @jax.named_scope('finish')
     def finish(c):
         u = slice(c * NI, (c + 1) * NI)
         a, b, d = e1[u], e4[u], e16[u]
@@ -321,6 +367,7 @@
             send(attl.at[c, :, pl.ds(poff, nj), :], lt.at[core, c], ds_l.at[c], dr_l.at[c], to_partner),
         )
 
+    @jax.named_scope('a_own')
     def a_own(c, copies):
         copies[0].wait_recv()
         part = ag.at[me, c]
@@ -329,6 +376,7 @@
             send(part, part, as_own.at[c, 1], ar_own.at[c, 1], to_lf),
         )
 
+    @jax.named_scope('a_fwd')
     def a_fwd(c, copies):
         copies[0].wait_recv()
         p0 = ag.at[lf, c, 0]
@@ -338,9 +386,11 @@
         f1 = send(p1, p1, as_fwd.at[c, 1], ar_fwd.at[c, 1], to_lf)
         return f0, f1
 
+    @jax.named_scope('a_mix')
     def a_mix(c, copies):
-        for f in copies:
-            f.wait_recv()
+        with jax.named_scope("af_wait"):
+            for f in copies:
+                f.wait_recv()
         lhs = jnp.concatenate([ag[s, c, h] for s in range(n_tp) for h in range(2)], axis=1)
         mm[c * rows : (c + 1) * rows, :] = dot(lhs, wcol[...]).astype(BF)
 
@@ -351,64 +401,70 @@
         there = ((t0 & (NC - 1)) == c) & (q0 == ((t0 >> 2) & (NI - 1)) * nj + (t0 >> 4))
         return jnp.where(there, 1.0, 0.0).astype(BF)
 
+    own_pair(2, pairs[2])
+    branch4(0)
+    pairs[3] = x_end(3, state[3])
+    w_start()
+    z_pass(0, 1)
     z_pass(1, 0)
+    branch4(1)
+    own_pair(3, pairs[3])
     z_pass(0, 2)
-    branch4(0)
     z_pass(1, 1)
-    branch4(1)
-    z_pass(0, 3)
     branch4(2)
     z_wait(2, 0)
     branch16(0)
+    z_pass(0, 3)
     z_pass(1, 2)
-    branch1(0)
-    branch1(1)
-    branch1(2)
+    for b in range(cj // 16):
+        branch1(b)
+    w_fwd = w_pass()
+    sent, own, fwd = {}, {}, {}
+    sent[0] = finish(0)
     branch4(3)
-    d0 = finish(0)
     z_wait(2, 1)
     branch16(1)
+    sent[1] = finish(1)
+    own[0] = a_own(0, sent[0])
     z_pass(1, 3)
-    d1 = finish(1)
-    w_fwd = w_pass()
-    a0 = a_own(0, d0)
-    a1 = a_own(1, d1)
-    f_0 = a_fwd(0, a0)
+    z_wait(2, 2)
+    branch16(2)
+    sent[2] = finish(2)
+    own[1] = a_own(1, sent[1])
+    fwd[0] = a_fwd(0, own[0])
+    z_wait(2, 3)
+    branch16(3)
+    sent[3] = finish(3)
+    own[2] = a_own(2, sent[2])
+    fwd[1] = a_fwd(1, own[1])
+    own[3] = a_own(3, sent[3])
     c_wo.wait()
     for f in w_fwd:
         f.wait_recv()
-    a_mix(0, f_0)
-    z_wait(2, 2)
-    branch16(2)
-    d2 = finish(2)
-    f_1 = a_fwd(1, a1)
-    a_mix(1, f_1)
-    a2 = a_own(2, d2)
-    z_wait(2, 3)
-    branch16(3)
-    d3 = finish(3)
-    f_2 = a_fwd(2, a2)
-    a3 = a_own(3, d3)
-    a_mix(2, f_2)
+    a_mix(0, fwd[0])
+    fwd[2] = a_fwd(2, own[2])
+    a_mix(1, fwd[1])
+    fwd[3] = a_fwd(3, own[3])
+    a_mix(2, fwd[2])
     macc[...] = sum(dot(back(c), mm[c * rows : (c + 1) * rows, :]) for c in range(3))
-    for d in (d0, d1, d2, d3):
+    for d in sent.values():
         d[1].wait_recv()
     lane = iota((1, hd), 1)
-    acc = jnp.zeros((tok, hd), F32)
+    acc = jnp.zeros((hd, tok), F32)
     for c in range(NC):
         x = jnp.where(lane == 0, lt[0, c].reshape(rows, hd), lt[1, c].reshape(rows, hd))
         hi = x.astype(BF)
         rest = x - hi.astype(F32)
         mid = rest.astype(BF)
         low = (rest - mid.astype(F32)).astype(BF)
-        p = back(c)
-        acc = acc + (dot(p, hi) + dot(p, mid) + dot(p, low))
-    log_ref[...] = acc[:, :2]
-    f_3 = a_fwd(3, a3)
-    a_mix(3, f_3)
+        p = perm[c * rows : (c + 1) * rows, :]
+        acc = acc + (dot_tn(hi, p) + dot_tn(mid, p) + dot_tn(low, p))
+    log_ref[...] = acc[:2, :]
+    a_mix(3, fwd[3])
     out_ref[...] = (macc[...] + dot(back(3), mm[3 * rows :, :])).astype(BF)
-    for copy in pending:
-        copy.wait_send()
+    with jax.named_scope("drain"):
+        for copy in pending:
+            copy.wait_send()
     for stage in range(3):
         @pl.when((z >= stage) & has_up)
         def _():
@@ -443,6 +499,10 @@
     vm = pltpu.VMEM
     scratch = [
         vm((tok, width), BF),
+        vm((n_tp * width // hd, hd), BF),
+        vm((n_tp, 1, width), F32),
+        vm((heads, hd), F32), vm((heads, hd), F32),
+        vm((1, 1, hd), F32), vm((1, 1, hd), F32),
         vm((n_tp, tok, width), BF),
         vm((n_tp * width, 6 * hd), BF),
         vm((tok, hd), F32), vm((tok, hd), F32),
@@ -463,7 +523,7 @@
         vm((2, NC, NI, nj, hd), F32),
         vm((tok, width), BF),
         vm((tok, width), F32),
-        dma((10,)),
+        dma((15,)),
         dma((NC, 2)), dma((NC, 2)), dma((NC, 2)), dma((NC, 2)),
         dma((NC,)), dma((NC,)),
         dma((3, NC)), dma((3, NC)),
@@ -471,25 +531,26 @@
         dma((NC,)), dma((NC,)), dma((NC,)), dma((NC,)),
         dma((NC, 2)), dma((NC, 2)), dma((NC, 2)), dma((NC, 2)),
     ]
-    hbm = pl.BlockSpec(memory_space=pl.ANY)
+    hbm = pl.BlockSpec(memory_space=pltpu.HBM)
     vmem = pl.BlockSpec(memory_space=pltpu.VMEM)
-    return pl.pallas_call(
+    mixed, logs = pl.pallas_call(
         functools.partial(kernel, n_tp, n_sp),
         out_shape=(
             jax.ShapeDtypeStruct((tok, width), BF),
-            jax.ShapeDtypeStruct((tok, heads), F32),
+            jax.ShapeDtypeStruct((heads, tok), F32),
         ),
-        in_specs=[hbm, vmem, hbm, hbm, hbm, vmem, vmem, hbm, hbm, hbm, vmem, vmem],
+        in_specs=[hbm] * 12,
         out_specs=(vmem, vmem),
         scratch_shapes=scratch,
         compiler_params=pltpu.CompilerParams(
-            collective_id=0, has_side_effects=True, vmem_limit_bytes=62 * 1024 * 1024
+            collective_id=0, has_side_effects=True, vmem_limit_bytes=63 * 1024 * 1024
         ),
     )(
-        hidden, norm_gain.astype(F32).reshape(n_tp, 1, width), w_query, w_key, w_value,
-        query_gain.reshape(heads, 1, hd), key_gain.reshape(heads, 1, hd), w_out,
-        jnp.asarray(tabc), jnp.asarray(tabs), jnp.asarray(basec), jnp.asarray(bases),
+        hidden, norm_gain.reshape(n_tp * width // hd, hd), w_query, w_key, w_value,
+        query_gain, key_gain, w_out,
+        jnp.asarray(tabc), jnp.asarray(tabs), jnp.asarray(basec)[:, None], jnp.asarray(bases)[:, None],
     )
+    return mixed, logs.T
 
 
 def solution(mesh):

time: 107 us -> 87 us (0.81)
  the two profiles are of different devices: /device:TPU:34 before, /device:TPU:160 now
where the time goes in v2:
time: 87 us; the launch traced here: 86.9 us
  Pallas kernels  83.9 us (96%)
  local copies, waits for them, and re-layouts  2.35 us (3%)
    pallas_call x1, Pallas kernels, local(): pl.pallas_call(functools.partial(kernel, n_tp, n_sp), out_shape=(jax.Shap...  83.9 us
    unnamed x4, local copies, waits for them, and re-layouts  2.35 us

profile of v2, /device:TPU:160, one launch (start us, length us, event | category | flops | bytes accessed | tf_op | source)
XLA Modules:
  0.0 86.9 jit_solution(5607326937986111959)
XLA Ops:
  0.6 83.9 %shard_map.131 = (bf16[384,512]{1,0:T(8,128)(2,1)}, f32[2,384]{1,0:T(2,128)}) custom-call(bf16[384,512]{1,0:T(8,128)(2,1)} %hid_h.1, bf16[16,128]{1,0:T(8,128)(2,1)} %bitcast.2, bf16[2048,256]{1,0:T(8,128)(2,1)} %wq_h.1, bf16[2048,256]{1,0:T(8,128)(2,1)} %wk_h.1, bf16[2048,256]{1,0:T(8,128)(2,1)} %wv_h.1, f32[2,128]{1,0:T(2,128)} %qg_h.1, f32[2,128]{1,0:T(2,128)} %kg_h.1, ...), custom_call_target="tpu_custom_call" | custom-call | tf_op jit(solution)/shard_map/pallas_call | solution.py:536
  84.5 0.0 copy-start
  84.5 1.8 %copy.16 = bf16[384,512]{1,0:T(8,128)(2,1)} copy(bf16[384,512]{1,0:T(8,128)(2,1)} %get-tuple-element.8) | data formatting | bytes 786432
  86.3 0.0 copy-done
  86.3 0.6 copy.17
Async XLA Ops:
  84.5 1.8 %copy-start = (f32[2,384]{1,0:T(2,128)S(1)}, f32[2,384]{1,0:T(2,128)}, u32[]{:S(2)}) copy-start(f32[2,384]{1,0:T(2,128)} %get-tuple-element.5) | copy-start | bytes 9220

commit v3 on v2

--- a/solution.py
+++ b/solution.py
@@ -38,13 +38,102 @@
     return lax.broadcasted_iota(jnp.int32, shape, dim)
 
 
+def early_kernel(
+    n_tp, hid_h, wo_h, hx_out, wc_out,
+    hid_v, hx, wcol, relay, lsem, xs_own, xr_own, xs_fwd, xr_fwd, ws, wr, osem,
+):
+    tok, width = hid_v.shape
+    half = tok // 2
+    wo_rows = wo_h.shape[0]
+    me = lax.axis_index("tp")
+    lf = lax.rem(me + n_tp - 1, n_tp)
+    rt = lax.rem(me + 1, n_tp)
+    op = lax.rem(me + 2, n_tp)
+
+    def remote(src, dst, ssem, rsem, to):
+        return pltpu.make_async_remote_copy(
+            src_ref=src, dst_ref=dst, send_sem=ssem, recv_sem=rsem,
+            device_id={"tp": to}, device_id_type=MESH,
+        )
+
+    def rows_of(ref, dev):
+        return ref.at[pl.ds(pl.multiple_of(dev * wo_rows, wo_rows), wo_rows), :]
+
+    def cols_of(dev):
+        return wo_h.at[:, pl.ds(pl.multiple_of(dev * width, width), width)]
+
+    @pl.when(lax.rem(lax.axis_index("sp"), 2) == 1)
+    def _():
+        c_hid = pltpu.make_async_copy(hid_h, hid_v, lsem.at[0])
+        c_hid.start()
+        barrier = pltpu.get_barrier_semaphore()
+        for dev in (rt, lf, op):
+            pl.semaphore_signal(barrier, inc=1, device_id={"tp": dev}, device_id_type=MESH)
+        c_wo = pltpu.make_async_copy(cols_of(me), rows_of(wcol, me), lsem.at[1])
+        c_wo.start()
+        perm = placement(tok)
+        c_hid.wait()
+        hx[me] = dot(perm, hid_v[...]).astype(BF)
+        pl.semaphore_wait(barrier, n_tp - 1)
+        own, fwd = [], []
+        for h in range(2):
+            part = hx.at[me, pl.ds(h * half, half), :]
+            own.append(remote(part, part, xs_own.at[h, 0], xr_own.at[h, 0], rt))
+            own.append(remote(part, part, xs_own.at[h, 1], xr_own.at[h, 1], lf))
+        for copy in own:
+            copy.start()
+        out = [remote(cols_of(dev), rows_of(wcol, me), ws.at[n], wr.at[n], dev) for n, dev in enumerate((rt, lf))]
+        wh = wo_rows // 2
+        turn, relayed = [], []
+        for n, (dev, src) in enumerate(((rt, lf), (lf, rt))):
+            part = wo_h.at[pl.ds(n * wh, wh), pl.ds(pl.multiple_of(op * width, width), width)]
+            turn.append(remote(part, relay.at[n], ws.at[2 + n], wr.at[2 + n], dev))
+            to = wcol.at[pl.ds(pl.multiple_of(src * wo_rows + n * wh, wh), wh), :]
+            relayed.append(remote(relay.at[n], to, ws.at[4 + n], wr.at[4 + n], dev))
+        for h in range(2):
+            lo = pl.ds(h * half, half // 2)
+            hi = pl.ds(h * half + half // 2, half // 2)
+            own[2 * h].wait_recv()
+            fwd.append(remote(hx.at[lf, lo, :], hx.at[lf, lo, :], xs_fwd.at[h, 0], xr_fwd.at[h, 0], rt))
+            fwd[-1].start()
+            own[2 * h + 1].wait_recv()
+            fwd.append(remote(hx.at[rt, hi, :], hx.at[rt, hi, :], xs_fwd.at[h, 1], xr_fwd.at[h, 1], lf))
+            fwd[-1].start()
+        for copy in turn + out:
+            copy.start()
+        for n in range(2):
+            turn[n].wait_recv()
+            relayed[n].start()
+        out = out + relayed
+        for copy in fwd:
+            copy.wait_recv()
+        o_hx = pltpu.make_async_copy(hx, hx_out, osem.at[0])
+        o_hx.start()
+        c_wo.wait()
+        for copy in out:
+            copy.wait_recv()
+        o_wc = pltpu.make_async_copy(wcol, wc_out, osem.at[1])
+        o_wc.start()
+        for copy in own + fwd + turn + out:
+            copy.wait_send()
+        o_hx.wait()
+        o_wc.wait()
+
+
+def placement(tok):
+    prow = iota((tok, tok), 0)
+    pcol = iota((tok, tok), 1)
+    place = (pcol & (NC - 1)) * (tok // NC) + ((pcol >> 2) & (NI - 1)) * (tok // WIDEST) + (pcol >> 4)
+    return jnp.where(prow == place, 1.0, 0.0).astype(BF)
+
+
 def kernel(
-    n_tp, n_sp,
-    hid_h, ng_h, wq_h, wk_h, wv_h, qg_h, kg_h, wo_h, tabc_h, tabs_h, basec_h, bases_h,
+    n_tp, n_sp, hxe_h, wce_h,
+    hid_h, ng_h, wq_h, wk_h, wv_h, qg_h, kg_h, tabc_h, tabs_h, basec_h, bases_h,
     out_ref, log_ref,
     hid_v, ng_v, ngain, qg_ref, kg_ref, basec, bases, hx, w_v, tabc, tabs, wcol, sbuf, fbuf, qb, kv, bias1, bias1e, bias4, bias16,
     o1, o4, o16, e1, e4, e16, attb, attl, attx, ag, lt, mm, macc,
-    lsem, xs_own, xr_own, xs_fwd, xr_fwd, ds_q, dr_q, zs, zr, ws, wr, wds, wdr,
+    lsem, xs_own, xr_own, xs_fwd, xr_fwd, ds_q, dr_q, zs, zr, ws, wr,
     ds_a, dr_a, ds_l, dr_l, as_own, ar_own, as_fwd, ar_fwd,
 ):
     tok, width = hid_v.shape
@@ -54,7 +143,6 @@
     cj = 2 * nj
     hd = KEYS_BEHIND
     depth = n_tp * width
-    wo_rows = wo_h.shape[0]
     own0 = kv.shape[2] - cj
     n_near = own0 - cj
     n_far = n_near - cj
@@ -76,14 +164,21 @@
     joff = pl.multiple_of(core * nj, 8)
     poff = pl.multiple_of(other * nj, 8)
 
+    first, second = core == 0, core == 1
     pending = []
 
-    def send(src, dst, ssem, rsem, dev):
+    def when(cond, f):
+        if cond is None:
+            f()
+        else:
+            pl.when(cond)(f)
+
+    def send(src, dst, ssem, rsem, dev, cond=None):
         copy = pltpu.make_async_remote_copy(
             src_ref=src, dst_ref=dst, send_sem=ssem, recv_sem=rsem, device_id=dev, device_id_type=MESH
         )
-        copy.start()
-        pending.append(copy)
+        when(cond, copy.start)
+        pending.append((cond, copy))
         return copy
 
     def load(src, dst, k):
@@ -91,19 +186,20 @@
         copy.start()
         return copy
 
-    c_hid = load(hid_h, hid_v, 0)
+    c_hid = pltpu.make_async_copy(hid_h, hid_v, lsem.at[0])
+    c_hx = pltpu.make_async_copy(hxe_h, hx, lsem.at[0])
+    c_wc = pltpu.make_async_copy(wce_h, wcol, lsem.at[9])
+    when(first, c_hid.start)
+    when(second, c_hx.start)
     for stage, (lo, hi) in enumerate(((n_near, own0), (n_far, n_near), (0, n_far))):
         @pl.when(z <= stage)
         def _():
             kv[:, :, lo:hi, :] = jnp.zeros((2, WIDEST, hi - lo, hd), BF)
     barrier = pltpu.get_barrier_semaphore()
-    for dev in (to_rt, to_lf, to_op, to_partner):
+    peers = [to_rt, to_lf, to_op, to_partner, {"tp": rt, "sp": partner}, {"tp": lf, "sp": partner}]
+    for dev in peers:
         pl.semaphore_signal(barrier, inc=1, device_id=dev, device_id_type=MESH)
     has_up, has_down = z < n_sp // 2 - 1, z > 0
-
-    @pl.when(has_up)
-    def _():
-        pl.semaphore_signal(barrier, inc=1, device_id=to_up, device_id_type=MESH)
 
     @pl.when(has_down)
     def _():
@@ -120,29 +216,27 @@
         ((ng_h, ng_v), (qg_h, qg_ref), (kg_h, kg_ref), (basec_h.at[pl.ds(sp, 1)], basec), (bases_h.at[pl.ds(sp, 1)], bases))
     ):
         c_t.append(load(src, dst, 10 + n))
-    my_cols = pl.ds(pl.multiple_of(me * width, width), width)
-    my_rows = pl.ds(pl.multiple_of(me * wo_rows, wo_rows), wo_rows)
-    c_wo = load(wo_h.at[:, my_cols], wcol.at[my_rows, :], 9)
-
-    prow = iota((tok, tok), 0)
-    pcol = iota((tok, tok), 1)
-    place = (pcol & (NC - 1)) * rows + ((pcol >> 2) & (NI - 1)) * nj + (pcol >> 4)
-    perm = jnp.where(prow == place, 1.0, 0.0).astype(BF)
-    with jax.named_scope("hid_wait"):
-        c_hid.wait()
-    mine = dot(perm, hid_v[...]).astype(BF)
-    hx[me] = mine
+    when(second, c_wc.start)
+
+    perm = placement(tok)
+
+    @pl.when(first)
+    def _():
+        with jax.named_scope("hid_wait"):
+            c_hid.wait()
+        hx[me] = dot(perm, hid_v[...]).astype(BF)
+
     with jax.named_scope("barrier_wait"):
-        pl.semaphore_wait(barrier, 4 + has_up.astype(jnp.int32) + has_down.astype(jnp.int32))
+        pl.semaphore_wait(barrier, len(peers) + has_up.astype(jnp.int32))
 
     def x_own(c):
         part = hx.at[me, pl.ds(c * rows, rows), :]
         return (
-            send(part, part, xs_own.at[c, 0], xr_own.at[c, 0], to_rt),
-            send(part, part, xs_own.at[c, 1], xr_own.at[c, 1], to_lf),
+            send(part, part, xs_own.at[c, 0], xr_own.at[c, 0], to_rt, first),
+            send(part, part, xs_own.at[c, 1], xr_own.at[c, 1], to_lf, first),
         )
 
-    x_sent = {0: x_own(0), 1: x_own(1)}
+    x_sent = {c: x_own(c) for c in range(NC)}
 
     for c in c_t:
         c.wait()
@@ -259,15 +353,13 @@
     def x_step(c):
         right, left = x_sent[c]
         with jax.named_scope("x_wait"):
-            right.wait_recv()
+            when(first, right.wait_recv)
         h0 = hx.at[lf, pl.ds(c * rows, half), :]
-        f0 = send(h0, h0, xs_fwd.at[c, 0], xr_fwd.at[c, 0], to_rt)
+        f0 = send(h0, h0, xs_fwd.at[c, 0], xr_fwd.at[c, 0], to_rt, first)
         with jax.named_scope("x_wait"):
-            left.wait_recv()
+            when(first, left.wait_recv)
         h1 = hx.at[rt, pl.ds(c * rows + half, half), :]
-        f1 = send(h1, h1, xs_fwd.at[c, 1], xr_fwd.at[c, 1], to_lf)
-        if c + 2 < NC:
-            x_sent[c + 2] = x_own(c + 2)
+        f1 = send(h1, h1, xs_fwd.at[c, 1], xr_fwd.at[c, 1], to_lf, first)
         acc = jnp.zeros((rows, 6 * hd), F32)
         sq = jnp.zeros((rows, 1), F32)
         for s in (me, lf, rt):
@@ -277,39 +369,13 @@
     def x_end(c, state):
         acc, sq, f0, f1 = state
         with jax.named_scope("xf_wait"):
-            f0.wait_recv()
-            f1.wait_recv()
+            when(first, f0.wait_recv)
+            when(first, f1.wait_recv)
         acc, sq = partial(c, op, acc, sq)
         return epilogue(c, acc, sq)
 
-    state, pairs = {}, {}
-    for c in range(NC):
-        state[c] = x_step(c)
-        if c >= 2:
-            own_pair(c - 2, pairs[c - 2])
-        if c >= 3:
-            z_pass(0, c - 3)
-        if c >= 1:
-            pairs[c - 1] = x_end(c - 1, state[c - 1])
-
-    wh = wo_rows // 2
-    w_sent = []
-
-    def w_start():
-        for n, dst in ((1, rt), (3, lf), (2, op)):
-            src = wo_h.at[pl.ds(pl.multiple_of(core * wh, wh), wh), pl.ds(pl.multiple_of(dst * width, width), width)]
-            to = wcol.at[pl.ds(pl.multiple_of(me * wo_rows + core * wh, wh), wh), :]
-            w_sent.append(send(src, to, ws.at[n - 1], wr.at[n - 1], {"tp": dst}))
-
-    @jax.named_scope('w_pass')
-    def w_pass():
-        fwd = []
-        for k, (n, src) in enumerate(((1, lf), (3, rt), (2, op))):
-            w_sent[k].wait_recv()
-            part = wcol.at[pl.ds(pl.multiple_of(src * wo_rows + core * wh, wh), wh), :]
-            fwd.append(send(part, part, wds.at[n - 1], wdr.at[n - 1], to_partner))
-        return fwd
-
+    with jax.named_scope("hx_wait"):
+        when(second, c_hx.wait)
     def softmax(s, bias):
         s = s * (hd ** -0.5) + bias
         m = jnp.max(s, axis=1, keepdims=True)
@@ -362,33 +428,33 @@
         attx[c] = attb[c, :, pl.ds(poff, nj), :].reshape(rows, hd).astype(BF)
         ag[me, c, core] = attb[c, :, pl.ds(joff, nj), :].reshape(rows, hd).astype(BF)
         lt[core, c] = attl[c, :, pl.ds(joff, nj), :]
-        return (
-            send(attx.at[c], ag.at[me, c, core], ds_a.at[c], dr_a.at[c], to_partner),
-            send(attl.at[c, :, pl.ds(poff, nj), :], lt.at[core, c], ds_l.at[c], dr_l.at[c], to_partner),
-        )
-
-    @jax.named_scope('a_own')
-    def a_own(c, copies):
-        copies[0].wait_recv()
-        part = ag.at[me, c]
-        return (
-            send(part, part, as_own.at[c, 0], ar_own.at[c, 0], to_rt),
-            send(part, part, as_own.at[c, 1], ar_own.at[c, 1], to_lf),
-        )
+        same, cross = ag.at[me, c, core], attx.at[c]
+        for side, dev in ((0, rt), (1, lf)):
+            send(same, same, as_own.at[c, side, 0], ar_own.at[c, side, core], {"tp": dev})
+            send(cross, same, as_own.at[c, side, 1], ar_own.at[c, side, core], {"tp": dev, "sp": partner})
+        send(cross, same, ds_a.at[c], dr_a.at[c], to_partner)
+        return send(attl.at[c, :, pl.ds(poff, nj), :], lt.at[core, c], ds_l.at[c], dr_l.at[c], to_partner)
+
+    def arrived(ref, sem):
+        pltpu.make_async_remote_copy(
+            src_ref=ref, dst_ref=ref, send_sem=sem, recv_sem=sem, device_id=to_partner, device_id_type=MESH
+        ).wait_recv()
 
     @jax.named_scope('a_fwd')
-    def a_fwd(c, copies):
-        copies[0].wait_recv()
-        p0 = ag.at[lf, c, 0]
+    def a_fwd(c):
+        p0, p1 = ag.at[lf, c, 0], ag.at[rt, c, 1]
+        arrived(p0, ar_own.at[c, 0, 0])
         f0 = send(p0, p0, as_fwd.at[c, 0], ar_fwd.at[c, 0], to_rt)
-        copies[1].wait_recv()
-        p1 = ag.at[rt, c, 1]
+        arrived(p1, ar_own.at[c, 1, 1])
         f1 = send(p1, p1, as_fwd.at[c, 1], ar_fwd.at[c, 1], to_lf)
         return f0, f1
 
     @jax.named_scope('a_mix')
     def a_mix(c, copies):
         with jax.named_scope("af_wait"):
+            arrived(ag.at[lf, c, 1], ar_own.at[c, 0, 1])
+            arrived(ag.at[rt, c, 0], ar_own.at[c, 1, 0])
+            arrived(ag.at[me, c, other], dr_a.at[c])
             for f in copies:
                 f.wait_recv()
         lhs = jnp.concatenate([ag[s, c, h] for s in range(n_tp) for h in range(2)], axis=1)
@@ -401,54 +467,66 @@
         there = ((t0 & (NC - 1)) == c) & (q0 == ((t0 >> 2) & (NI - 1)) * nj + (t0 >> 4))
         return jnp.where(there, 1.0, 0.0).astype(BF)
 
-    own_pair(2, pairs[2])
-    branch4(0)
+    state, pairs = {}, {}
+    edge = z == 0
+
+    def early(c):
+        @pl.when(edge & first)
+        def _():
+            branch16(c)
+            branch4(c)
+
+    for c in range(NC):
+        state[c] = x_step(c)
+        if c >= 2:
+            pl.when(first)(functools.partial(own_pair, c - 2, pairs[c - 2]))
+        if c >= 3:
+            early(c - 3)
+        if c >= 1:
+            pairs[c - 1] = x_end(c - 1, state[c - 1])
+    pl.when(first)(functools.partial(own_pair, 2, pairs[2]))
+    early(1)
     pairs[3] = x_end(3, state[3])
-    w_start()
+    when(second, c_wc.wait)
+    c_w = send(wcol, wcol, ws.at[0], wr.at[0], to_partner, second)
+    early(2)
+    for c in range(3):
+        pl.when(second)(functools.partial(own_pair, c, pairs[c]))
+
+        @pl.when(edge & second)
+        def _():
+            branch16(c)
+            branch4(c)
+
+    own_pair(3, pairs[3])
+    z_pass(0, 0)
     z_pass(0, 1)
-    z_pass(1, 0)
-    branch4(1)
-    own_pair(3, pairs[3])
-    z_pass(0, 2)
-    z_pass(1, 1)
-    branch4(2)
-    z_wait(2, 0)
-    branch16(0)
-    z_pass(0, 3)
-    z_pass(1, 2)
+    for c in range(3):
+        pl.when(~edge)(functools.partial(branch4, c))
+        if c + 2 < NC:
+            z_pass(0, c + 2)
     for b in range(cj // 16):
         branch1(b)
-    w_fwd = w_pass()
-    sent, own, fwd = {}, {}, {}
-    sent[0] = finish(0)
+    for c in range(NC):
+        z_pass(1, c)
     branch4(3)
-    z_wait(2, 1)
-    branch16(1)
-    sent[1] = finish(1)
-    own[0] = a_own(0, sent[0])
-    z_pass(1, 3)
-    z_wait(2, 2)
-    branch16(2)
-    sent[2] = finish(2)
-    own[1] = a_own(1, sent[1])
-    fwd[0] = a_fwd(0, own[0])
-    z_wait(2, 3)
-    branch16(3)
-    sent[3] = finish(3)
-    own[2] = a_own(2, sent[2])
-    fwd[1] = a_fwd(1, own[1])
-    own[3] = a_own(3, sent[3])
-    c_wo.wait()
-    for f in w_fwd:
-        f.wait_recv()
-    a_mix(0, fwd[0])
-    fwd[2] = a_fwd(2, own[2])
-    a_mix(1, fwd[1])
-    fwd[3] = a_fwd(3, own[3])
-    a_mix(2, fwd[2])
+    logs_sent, fwd = {}, {}
+    for c in range(NC):
+        z_wait(2, c)
+        if c == 3:
+            branch16(c)
+        else:
+            pl.when(~edge)(functools.partial(branch16, c))
+        logs_sent[c] = finish(c)
+    for c in range(NC):
+        fwd[c] = a_fwd(c)
+    with jax.named_scope("w_wait"):
+        when(first, c_w.wait_recv)
+    for c in range(3):
+        a_mix(c, fwd[c])
     macc[...] = sum(dot(back(c), mm[c * rows : (c + 1) * rows, :]) for c in range(3))
-    for d in sent.values():
-        d[1].wait_recv()
+    for copy in logs_sent.values():
+        copy.wait_recv()
     lane = iota((1, hd), 1)
     acc = jnp.zeros((hd, tok), F32)
     for c in range(NC):
@@ -463,8 +541,8 @@
     a_mix(3, fwd[3])
     out_ref[...] = (macc[...] + dot(back(3), mm[3 * rows :, :])).astype(BF)
     with jax.named_scope("drain"):
-        for copy in pending:
-            copy.wait_send()
+        for cond, copy in pending:
+            when(cond, copy.wait_send)
     for stage in range(3):
         @pl.when((z >= stage) & has_up)
         def _():
@@ -527,27 +605,44 @@
         dma((NC, 2)), dma((NC, 2)), dma((NC, 2)), dma((NC, 2)),
         dma((NC,)), dma((NC,)),
         dma((3, NC)), dma((3, NC)),
-        dma((3,)), dma((3,)), dma((3,)), dma((3,)),
+        dma((1,)), dma((1,)),
         dma((NC,)), dma((NC,)), dma((NC,)), dma((NC,)),
-        dma((NC, 2)), dma((NC, 2)), dma((NC, 2)), dma((NC, 2)),
+        dma((NC, 2, 2)), dma((NC, 2, 2)), dma((NC, 2)), dma((NC, 2)),
     ]
     hbm = pl.BlockSpec(memory_space=pltpu.HBM)
     vmem = pl.BlockSpec(memory_space=pltpu.VMEM)
+    early_hx, early_wc = pl.pallas_call(
+        functools.partial(early_kernel, n_tp),
+        out_shape=(
+            jax.ShapeDtypeStruct((n_tp, tok, width), BF),
+            jax.ShapeDtypeStruct((n_tp * heads * hd, width), BF),
+        ),
+        in_specs=[hbm] * 2,
+        out_specs=(hbm, hbm),
+        scratch_shapes=[
+            vm((tok, width), BF), vm((n_tp, tok, width), BF), vm((n_tp * heads * hd, width), BF),
+            vm((2, heads * hd // 2, width), BF),
+            dma((2,)), dma((2, 2)), dma((2, 2)), dma((2, 2)), dma((2, 2)), dma((6,)), dma((6,)), dma((2,)),
+        ],
+        compiler_params=pltpu.CompilerParams(
+            collective_id=1, has_side_effects=True, vmem_limit_bytes=63 * 1024 * 1024
+        ),
+    )(hidden, w_out)
     mixed, logs = pl.pallas_call(
         functools.partial(kernel, n_tp, n_sp),
         out_shape=(
             jax.ShapeDtypeStruct((tok, width), BF),
             jax.ShapeDtypeStruct((heads, tok), F32),
         ),
-        in_specs=[hbm] * 12,
+        in_specs=[hbm] * 13,
         out_specs=(vmem, vmem),
         scratch_shapes=scratch,
         compiler_params=pltpu.CompilerParams(
             collective_id=0, has_side_effects=True, vmem_limit_bytes=63 * 1024 * 1024
         ),
     )(
-        hidden, norm_gain.reshape(n_tp * width // hd, hd), w_query, w_key, w_value,
-        query_gain, key_gain, w_out,
+        early_hx, early_wc, hidden, norm_gain.reshape(n_tp * width // hd, hd), w_query, w_key, w_value,
+        query_gain, key_gain,
         jnp.asarray(tabc), jnp.asarray(tabs), jnp.asarray(basec)[:, None], jnp.asarray(bases)[:, None],
     )
     return mixed, logs.T

time: 87 us -> 80.9 us (0.930)
  Pallas kernels: 83.9 us -> 77 us
    pallas_call x1, Pallas kernels: 83.9 us -> 76 us  [local(): pl.pallas_call(functools.partial(kernel, n_tp, n_sp), out_shape=(jax.Shap...]
    pallas_call x0 -> x1, Pallas kernels: none -> 1 us  [local(): pl.pallas_call(functools.partial(early_kernel, n_tp), out_shape=(jax.Shap...]
    unnamed x4 -> x2, local copies, waits for them, and re-layouts: 2.35 us -> 3.02 us
where the time goes in v3:
time: 80.9 us; the launch traced here: 80.7 us
  Pallas kernels  77 us (95%)
  local copies, waits for them, and re-layouts  3.02 us (4%)
    pallas_call x1, Pallas kernels, local(): pl.pallas_call(functools.partial(kernel, n_tp, n_sp), out_shape=(jax.Shap...  76 us
    unnamed x2, local copies, waits for them, and re-layouts  3.02 us

profile of v3, /device:TPU:160, one launch (start us, length us, event | category | flops | bytes accessed | tf_op | source)
XLA Modules:
  0.0 80.7 jit_solution(12620064405878648529)
XLA Ops:
  0.6 1.0 %shard_map.131 = (bf16[4,384,512]{2,1,0:T(8,128)(2,1)}, bf16[1024,512]{1,0:T(8,128)(2,1)}) custom-call(bf16[384,512]{1,0:T(8,128)(2,1)} %hid_h.3, bf16[256,2048]{1,0:T(8,128)(2,1)} %wo_h.1), custom_call_target="tpu_custom_call" | custom-call | tf_op jit(solution)/shard_map/pallas_call | solution.py:614
  1.6 76.0 %shard_map.132 = (bf16[384,512]{1,0:T(8,128)(2,1)}, f32[2,384]{1,0:T(2,128)}) custom-call(bf16[4,384,512]{2,1,0:T(8,128)(2,1)} %get-tuple-element.6.hxe_h, bf16[1024,512]{1,0:T(8,128)(2,1)} %get-tuple-element.7.wce_h, bf16[384,512]{1,0:T(8,128)(2,1)} %hid_h.3, bf16[16,128]{1,0:T(8,128)(2,1)} %bitcast.2, bf16[2048,256]{1,0:T(8,128)(2,1)} %wq_h.1, ...), custom_call_target="tpu_custom_call" | custom-call | tf_op jit(solution)/shard_map/pallas_call | solution.py:631
  77.7 1.8 %copy.16 = bf16[384,512]{1,0:T(8,128)(2,1)} copy(bf16[384,512]{1,0:T(8,128)(2,1)} %get-tuple-element.12) | data formatting | bytes 786432
  79.4 1.3 %copy.17 = f32[384,2]{0,1:T(2,128)} copy(f32[384,2]{0,1:T(2,128)} %bitcast.3) | data formatting | bytes 6144

commit v4 on v3

--- a/solution.py
+++ b/solution.py
@@ -134,7 +134,7 @@
     hid_v, ng_v, ngain, qg_ref, kg_ref, basec, bases, hx, w_v, tabc, tabs, wcol, sbuf, fbuf, qb, kv, bias1, bias1e, bias4, bias16,
     o1, o4, o16, e1, e4, e16, attb, attl, attx, ag, lt, mm, macc,
     lsem, xs_own, xr_own, xs_fwd, xr_fwd, ds_q, dr_q, zs, zr, ws, wr,
-    ds_a, dr_a, ds_l, dr_l, as_own, ar_own, as_fwd, ar_fwd,
+    ds_a, dr_a, ds_l, dr_l, as_own, ar_own, as_fwd, ar_fwd, as_op, ar_op,
 ):
     tok, width = hid_v.shape
     rows = tok // NC
@@ -189,14 +189,11 @@
     c_hid = pltpu.make_async_copy(hid_h, hid_v, lsem.at[0])
     c_hx = pltpu.make_async_copy(hxe_h, hx, lsem.at[0])
     c_wc = pltpu.make_async_copy(wce_h, wcol, lsem.at[9])
-    when(first, c_hid.start)
-    when(second, c_hx.start)
-    for stage, (lo, hi) in enumerate(((n_near, own0), (n_far, n_near), (0, n_far))):
-        @pl.when(z <= stage)
-        def _():
-            kv[:, :, lo:hi, :] = jnp.zeros((2, WIDEST, hi - lo, hd), BF)
     barrier = pltpu.get_barrier_semaphore()
-    peers = [to_rt, to_lf, to_op, to_partner, {"tp": rt, "sp": partner}, {"tp": lf, "sp": partner}]
+    peers = [
+        to_rt, to_lf, to_op, to_partner,
+        {"tp": rt, "sp": partner}, {"tp": lf, "sp": partner}, {"tp": op, "sp": partner},
+    ]
     for dev in peers:
         pl.semaphore_signal(barrier, inc=1, device_id=dev, device_id_type=MESH)
     has_up, has_down = z < n_sp // 2 - 1, z > 0
@@ -205,6 +202,8 @@
     def _():
         pl.semaphore_signal(barrier, inc=1, device_id=to_down, device_id_type=MESH)
 
+    when(first, c_hid.start)
+    when(second, c_hx.start)
     own_col = pl.ds(pl.multiple_of(core * hd, hd), hd)
     oth_col = pl.ds(pl.multiple_of(other * hd, hd), hd)
     c_w = []
@@ -237,6 +236,11 @@
         )
 
     x_sent = {c: x_own(c) for c in range(NC)}
+
+    for stage, (lo, hi) in enumerate(((n_near, own0), (n_far, n_near), (0, n_far))):
+        @pl.when(z <= stage)
+        def _():
+            kv[:, :, lo:hi, :] = jnp.zeros((2, WIDEST, hi - lo, hd), BF)
 
     for c in c_t:
         c.wait()
@@ -317,40 +321,42 @@
     ):
         for c in range(NC):
             u = pl.ds(c * NI, NI)
-            z_copies[stage, c] = pltpu.make_async_remote_copy(
-                src_ref=kv.at[:, u, pl.ds(start, count), :], dst_ref=kv.at[:, u, pl.ds(to, count), :],
-                send_sem=zs.at[stage, c], recv_sem=zr.at[stage, c], device_id=to_up, device_id_type=MESH,
-            )
-
-    def z_send(stage, c):
-        @pl.when((z >= stage) & has_up)
-        def _():
-            z_copies[stage, c].start()
+            z_copies[stage, c] = [
+                pltpu.make_async_remote_copy(
+                    src_ref=kv.at[n, u, pl.ds(start, count), :], dst_ref=kv.at[n, u, pl.ds(to, count), :],
+                    send_sem=zs.at[stage, c, n], recv_sem=zr.at[stage, c, n],
+                    device_id=to_up, device_id_type=MESH,
+                )
+                for n in range(2)
+            ]
+
+    def z_send(stage, c, n):
+        when((z >= stage) & has_up, z_copies[stage, c][n].start)
 
     @jax.named_scope('z_wait')
     def z_wait(stage, c):
-        @pl.when(z > stage)
-        def _():
-            z_copies[stage, c].wait_recv()
+        for n in range(2):
+            when(z > stage, z_copies[stage, c][n].wait_recv)
 
     @jax.named_scope('z_pass')
     def z_pass(stage, c):
-        z_wait(stage, c)
-        z_send(stage + 1, c)
+        for n in range(2):
+            when(z > stage, z_copies[stage, c][n].wait_recv)
+            z_send(stage + 1, c, n)
 
     @jax.named_scope('own_pair')
     def own_pair(c, copy):
         with jax.named_scope("pair_wait"):
             copy.wait_recv()
         u = slice(c * NI, (c + 1) * NI)
-        kv[0, u, own0:, :] = fbuf[1, u].astype(BF)
-        kv[1, u, own0:, :] = fbuf[2, u].astype(BF)
-        z_send(0, c)
+        for n in range(2):
+            kv[n, u, own0:, :] = fbuf[1 + n, u].astype(BF)
+            z_send(0, c, n)
         qb[u] = fbuf[0, u].astype(BF)
 
     for c in c_w:
         c.wait()
-    def x_step(c):
+    def x_pass(c):
         right, left = x_sent[c]
         with jax.named_scope("x_wait"):
             when(first, right.wait_recv)
@@ -360,11 +366,14 @@
             when(first, left.wait_recv)
         h1 = hx.at[rt, pl.ds(c * rows + half, half), :]
         f1 = send(h1, h1, xs_fwd.at[c, 1], xr_fwd.at[c, 1], to_lf, first)
+        return f0, f1
+
+    def x_near(c, passed):
         acc = jnp.zeros((rows, 6 * hd), F32)
         sq = jnp.zeros((rows, 1), F32)
         for s in (me, lf, rt):
             acc, sq = partial(c, s, acc, sq)
-        return acc, sq, f0, f1
+        return acc, sq, *passed
 
     def x_end(c, state):
         acc, sq, f0, f1 = state
@@ -432,6 +441,9 @@
         for side, dev in ((0, rt), (1, lf)):
             send(same, same, as_own.at[c, side, 0], ar_own.at[c, side, core], {"tp": dev})
             send(cross, same, as_own.at[c, side, 1], ar_own.at[c, side, core], {"tp": dev, "sp": partner})
+        if c == NC - 1:
+            send(same, same, as_op.at[0], ar_op.at[core], to_op)
+            send(cross, same, as_op.at[1], ar_op.at[core], {"tp": op, "sp": partner})
         send(cross, same, ds_a.at[c], dr_a.at[c], to_partner)
         return send(attl.at[c, :, pl.ds(poff, nj), :], lt.at[core, c], ds_l.at[c], dr_l.at[c], to_partner)
 
@@ -455,8 +467,14 @@
             arrived(ag.at[lf, c, 1], ar_own.at[c, 0, 1])
             arrived(ag.at[rt, c, 0], ar_own.at[c, 1, 0])
             arrived(ag.at[me, c, other], dr_a.at[c])
-            for f in copies:
-                f.wait_recv()
+            if c < NC - 1:
+                for f in copies:
+                    f.wait_recv()
+            else:
+                arrived(ag.at[lf, c, 0], ar_own.at[c, 0, 0])
+                arrived(ag.at[rt, c, 1], ar_own.at[c, 1, 1])
+                for h in range(2):
+                    arrived(ag.at[op, c, h], ar_op.at[h])
         lhs = jnp.concatenate([ag[s, c, h] for s in range(n_tp) for h in range(2)], axis=1)
         mm[c * rows : (c + 1) * rows, :] = dot(lhs, wcol[...]).astype(BF)
 
@@ -476,50 +494,60 @@
             branch16(c)
             branch4(c)
 
-    for c in range(NC):
-        state[c] = x_step(c)
-        if c >= 2:
-            pl.when(first)(functools.partial(own_pair, c - 2, pairs[c - 2]))
-        if c >= 3:
-            early(c - 3)
-        if c >= 1:
-            pairs[c - 1] = x_end(c - 1, state[c - 1])
-    pl.when(first)(functools.partial(own_pair, 2, pairs[2]))
-    early(1)
+    def pair_first(c):
+        pl.when(first)(functools.partial(own_pair, c, pairs[c]))
+
+    passed = {0: x_pass(0), 1: x_pass(1)}
+    state[0] = x_near(0, passed[0])
+    passed[2] = x_pass(2)
+    state[1] = x_near(1, passed[1])
+    passed[3] = x_pass(3)
+    pairs[0] = x_end(0, state[0])
+    state[2] = x_near(2, passed[2])
+    pair_first(0)
+    pairs[1] = x_end(1, state[1])
+    state[3] = x_near(3, passed[3])
+    pair_first(1)
+    pairs[2] = x_end(2, state[2])
     pairs[3] = x_end(3, state[3])
+    pair_first(2)
     when(second, c_wc.wait)
     c_w = send(wcol, wcol, ws.at[0], wr.at[0], to_partner, second)
-    early(2)
+    early(0)
     for c in range(3):
         pl.when(second)(functools.partial(own_pair, c, pairs[c]))
 
-        @pl.when(edge & second)
-        def _():
-            branch16(c)
-            branch4(c)
-
+    pl.when(edge & second)(functools.partial(branch4, 0))
     own_pair(3, pairs[3])
     z_pass(0, 0)
     z_pass(0, 1)
-    for c in range(3):
+    for c in range(2):
         pl.when(~edge)(functools.partial(branch4, c))
-        if c + 2 < NC:
-            z_pass(0, c + 2)
+        pl.when(z == 1)(functools.partial(branch16, c))
+        z_pass(0, c + 2)
     for b in range(cj // 16):
         branch1(b)
     for c in range(NC):
         z_pass(1, c)
-    branch4(3)
+        if c < 2:
+            pl.when(z == 2)(functools.partial(branch16, c))
     logs_sent, fwd = {}, {}
     for c in range(NC):
         z_wait(2, c)
-        if c == 3:
+        if c < 2:
+            pl.when((z > 2) | (edge & (second | (c > 0))))(functools.partial(branch16, c))
+            if c > 0:
+                pl.when(edge)(functools.partial(branch4, c))
+        else:
+            if c == 2:
+                branch4(2)
             branch16(c)
-        else:
-            pl.when(~edge)(functools.partial(branch16, c))
         logs_sent[c] = finish(c)
-    for c in range(NC):
+        if c == 2:
+            branch4(3)
+    for c in range(NC - 1):
         fwd[c] = a_fwd(c)
+    fwd[NC - 1] = ()
     with jax.named_scope("w_wait"):
         when(first, c_w.wait_recv)
     for c in range(3):
@@ -547,7 +575,8 @@
         @pl.when((z >= stage) & has_up)
         def _():
             for c in range(NC):
-                z_copies[stage, c].wait_send()
+                for n in range(2):
+                    z_copies[stage, c][n].wait_send()
 
 
 def tables(tok, n_sp, hd):
@@ -604,10 +633,10 @@
         dma((15,)),
         dma((NC, 2)), dma((NC, 2)), dma((NC, 2)), dma((NC, 2)),
         dma((NC,)), dma((NC,)),
-        dma((3, NC)), dma((3, NC)),
+        dma((3, NC, 2)), dma((3, NC, 2)),
         dma((1,)), dma((1,)),
         dma((NC,)), dma((NC,)), dma((NC,)), dma((NC,)),
-        dma((NC, 2, 2)), dma((NC, 2, 2)), dma((NC, 2)), dma((NC, 2)),
+        dma((NC, 2, 2)), dma((NC, 2, 2)), dma((NC - 1, 2)), dma((NC - 1, 2)), dma((2,)), dma((2,)),
     ]
     hbm = pl.BlockSpec(memory_space=pltpu.HBM)
     vmem = pl.BlockSpec(memory_space=pltpu.VMEM)
@@ -631,8 +660,8 @@
     mixed, logs = pl.pallas_call(
         functools.partial(kernel, n_tp, n_sp),
         out_shape=(
-            jax.ShapeDtypeStruct((tok, width), BF),
-            jax.ShapeDtypeStruct((heads, tok), F32),
+            pltpu.VMEM((tok, width), BF),
+            pltpu.VMEM((heads, tok), F32),
         ),
         in_specs=[hbm] * 13,
         out_specs=(vmem, vmem),

time: 80.9 us -> 77.9 us (0.963)
  the two profiles are of different devices: /device:TPU:160 before, /device:TPU:96 now
where the time goes in v4:
time: 77.9 us; the launch traced here: 77.8 us
  Pallas kernels  75.8 us (97%)
  local copies, waits for them, and re-layouts  1.33 us (2%)
    pallas_call x1, Pallas kernels, local(): pl.pallas_call(functools.partial(kernel, n_tp, n_sp), out_shape=(pltpu.VM...  74.8 us

profile of v4, /device:TPU:96, one launch (start us, length us, event | category | flops | bytes accessed | tf_op | source)
XLA Modules:
  0.0 77.8 jit_solution(11146982903624830884)
XLA Ops:
  0.6 1.0 %shard_map.131 = (bf16[4,384,512]{2,1,0:T(8,128)(2,1)}, bf16[1024,512]{1,0:T(8,128)(2,1)}) custom-call(bf16[384,512]{1,0:T(8,128)(2,1)} %hid_h.3, bf16[256,2048]{1,0:T(8,128)(2,1)} %wo_h.1), custom_call_target="tpu_custom_call" | custom-call | tf_op jit(solution)/shard_map/pallas_call | solution.py:643
  1.6 74.8 %shard_map.132 = (bf16[384,512]{1,0:T(8,128)(2,1)S(1)}, f32[2,384]{1,0:T(2,128)S(1)}) custom-call(bf16[4,384,512]{2,1,0:T(8,128)(2,1)} %get-tuple-element.6.hxe_h, bf16[1024,512]{1,0:T(8,128)(2,1)} %get-tuple-element.7.wce_h, bf16[384,512]{1,0:T(8,128)(2,1)} %hid_h.3, bf16[16,128]{1,0:T(8,128)(2,1)} %bitcast.3, bf16[2048,256]{1,0:T(8,128)(2,1)} %wq_h.1, ...), custom_call_target="tpu_custom_call" | custom-call | tf_op jit(solution)/shard_map/pallas_call | solution.py:660
  76.4 0.7 copy.16
  77.2 0.6 copy.17

commit v5 on v4

--- a/solution.py
+++ b/solution.py
@@ -437,29 +437,55 @@
         attx[c] = attb[c, :, pl.ds(poff, nj), :].reshape(rows, hd).astype(BF)
         ag[me, c, core] = attb[c, :, pl.ds(joff, nj), :].reshape(rows, hd).astype(BF)
         lt[core, c] = attl[c, :, pl.ds(joff, nj), :]
+        for copy in plans[c]:
+            copy.start()
+
+    def finish_plan(c):
         same, cross = ag.at[me, c, core], attx.at[c]
+        copies = []
+
+        def add(src, dst, ssem, rsem, dev):
+            copies.append(
+                pltpu.make_async_remote_copy(
+                    src_ref=src, dst_ref=dst, send_sem=ssem, recv_sem=rsem, device_id=dev, device_id_type=MESH
+                )
+            )
+            pending.append((None, copies[-1]))
+
         for side, dev in ((0, rt), (1, lf)):
-            send(same, same, as_own.at[c, side, 0], ar_own.at[c, side, core], {"tp": dev})
-            send(cross, same, as_own.at[c, side, 1], ar_own.at[c, side, core], {"tp": dev, "sp": partner})
+            add(same, same, as_own.at[c, side, 0], ar_own.at[c, side, core], {"tp": dev})
+            add(cross, same, as_own.at[c, side, 1], ar_own.at[c, side, core], {"tp": dev, "sp": partner})
         if c == NC - 1:
-            send(same, same, as_op.at[0], ar_op.at[core], to_op)
-            send(cross, same, as_op.at[1], ar_op.at[core], {"tp": op, "sp": partner})
-        send(cross, same, ds_a.at[c], dr_a.at[c], to_partner)
-        return send(attl.at[c, :, pl.ds(poff, nj), :], lt.at[core, c], ds_l.at[c], dr_l.at[c], to_partner)
+            add(same, same, as_op.at[0], ar_op.at[core], to_op)
+            add(cross, same, as_op.at[1], ar_op.at[core], {"tp": op, "sp": partner})
+        add(cross, same, ds_a.at[c], dr_a.at[c], to_partner)
+        add(attl.at[c, :, pl.ds(poff, nj), :], lt.at[core, c], ds_l.at[c], dr_l.at[c], to_partner)
+        return copies
 
     def arrived(ref, sem):
         pltpu.make_async_remote_copy(
             src_ref=ref, dst_ref=ref, send_sem=sem, recv_sem=sem, device_id=to_partner, device_id_type=MESH
         ).wait_recv()
 
+    def a_plan(c):
+        p0, p1 = ag.at[lf, c, 0], ag.at[rt, c, 1]
+        f0 = pltpu.make_async_remote_copy(
+            src_ref=p0, dst_ref=p0, send_sem=as_fwd.at[c, 0], recv_sem=ar_fwd.at[c, 0],
+            device_id=to_rt, device_id_type=MESH,
+        )
+        f1 = pltpu.make_async_remote_copy(
+            src_ref=p1, dst_ref=p1, send_sem=as_fwd.at[c, 1], recv_sem=ar_fwd.at[c, 1],
+            device_id=to_lf, device_id_type=MESH,
+        )
+        pending.extend([(None, f0), (None, f1)])
+        return f0, f1
+
     @jax.named_scope('a_fwd')
-    def a_fwd(c):
-        p0, p1 = ag.at[lf, c, 0], ag.at[rt, c, 1]
-        arrived(p0, ar_own.at[c, 0, 0])
-        f0 = send(p0, p0, as_fwd.at[c, 0], ar_fwd.at[c, 0], to_rt)
-        arrived(p1, ar_own.at[c, 1, 1])
-        f1 = send(p1, p1, as_fwd.at[c, 1], ar_fwd.at[c, 1], to_lf)
-        return f0, f1
+    def a_fwd(c, copies):
+        arrived(ag.at[lf, c, 0], ar_own.at[c, 0, 0])
+        copies[0].start()
+        arrived(ag.at[rt, c, 1], ar_own.at[c, 1, 1])
+        copies[1].start()
 
     @jax.named_scope('a_mix')
     def a_mix(c, copies):
@@ -497,18 +523,13 @@
     def pair_first(c):
         pl.when(first)(functools.partial(own_pair, c, pairs[c]))
 
-    passed = {0: x_pass(0), 1: x_pass(1)}
-    state[0] = x_near(0, passed[0])
-    passed[2] = x_pass(2)
-    state[1] = x_near(1, passed[1])
-    passed[3] = x_pass(3)
+    for c in range(NC):
+        state[c] = x_near(c, x_pass(c))
     pairs[0] = x_end(0, state[0])
-    state[2] = x_near(2, passed[2])
+    pairs[1] = x_end(1, state[1])
     pair_first(0)
-    pairs[1] = x_end(1, state[1])
-    state[3] = x_near(3, passed[3])
+    pairs[2] = x_end(2, state[2])
     pair_first(1)
-    pairs[2] = x_end(2, state[2])
     pairs[3] = x_end(3, state[3])
     pair_first(2)
     when(second, c_wc.wait)
@@ -519,42 +540,53 @@
 
     pl.when(edge & second)(functools.partial(branch4, 0))
     own_pair(3, pairs[3])
-    z_pass(0, 0)
-    z_pass(0, 1)
-    for c in range(2):
+    for b in range(1, cj // 16):
+        branch1(b)
+    plans = [finish_plan(c) for c in range(NC)]
+    fwd = {c: a_plan(c) for c in range(NC - 1)}
+    for c in range(3):
+        z_pass(0, c)
         pl.when(~edge)(functools.partial(branch4, c))
         pl.when(z == 1)(functools.partial(branch16, c))
-        z_pass(0, c + 2)
-    for b in range(cj // 16):
-        branch1(b)
+    z_pass(0, 3)
+    branch1(0)
+    pl.when(z >= 2)(functools.partial(branch4, 3))
     for c in range(NC):
         z_pass(1, c)
-        if c < 2:
-            pl.when(z == 2)(functools.partial(branch16, c))
-    logs_sent, fwd = {}, {}
-    for c in range(NC):
-        z_wait(2, c)
-        if c < 2:
-            pl.when((z > 2) | (edge & (second | (c > 0))))(functools.partial(branch16, c))
-            if c > 0:
+
+        @pl.when(z == 2)
+        def _():
+            branch16(c)
+            finish(c)
+
+    @pl.when(z != 2)
+    def _():
+        for c in range(NC):
+            z_wait(2, c)
+
+            @pl.when((z > 2) | (edge & (second | (c > 0))) | (c == 3))
+            def _():
+                branch16(c)
+
+            if c == 3:
+                pl.when(z < 2)(functools.partial(branch4, c))
+            elif c > 0:
                 pl.when(edge)(functools.partial(branch4, c))
-        else:
+            finish(c)
             if c == 2:
-                branch4(2)
-            branch16(c)
-        logs_sent[c] = finish(c)
-        if c == 2:
-            branch4(3)
-    for c in range(NC - 1):
-        fwd[c] = a_fwd(c)
+                pl.when(z > 2)(functools.partial(a_fwd, 0, fwd[0]))
+
+    pl.when(z <= 2)(functools.partial(a_fwd, 0, fwd[0]))
+    for c in range(1, NC - 1):
+        a_fwd(c, fwd[c])
     fwd[NC - 1] = ()
     with jax.named_scope("w_wait"):
         when(first, c_w.wait_recv)
     for c in range(3):
         a_mix(c, fwd[c])
     macc[...] = sum(dot(back(c), mm[c * rows : (c + 1) * rows, :]) for c in range(3))
-    for copy in logs_sent.values():
-        copy.wait_recv()
+    for c in range(NC):
+        plans[c][-1].wait_recv()
     lane = iota((1, hd), 1)
     acc = jnp.zeros((hd, tok), F32)
     for c in range(NC):

time: 77.9 us -> 77.1 us (0.990)
  Pallas kernels: 75.8 us -> 75 us
    pallas_call x1, Pallas kernels: 74.8 us -> 74 us  [local(): pl.pallas_call(functools.partial(kernel, n_tp, n_sp), out_shape=(pltpu.VM...]
where the time goes in v5:
time: 77.1 us; the launch traced here: 77 us
  Pallas kernels  75 us (97%)
  local copies, waits for them, and re-layouts  1.33 us (2%)
    pallas_call x1, Pallas kernels, local(): pl.pallas_call(functools.partial(kernel, n_tp, n_sp), out_shape=(pltpu.VM...  74 us

profile of v5, /device:TPU:96, one launch (start us, length us, event | category | flops | bytes accessed | tf_op | source)
XLA Modules:
  0.0 77.0 jit_solution(10618139478225910847)
XLA Ops:
  0.6 1.0 %shard_map.131 = (bf16[4,384,512]{2,1,0:T(8,128)(2,1)}, bf16[1024,512]{1,0:T(8,128)(2,1)}) custom-call(bf16[384,512]{1,0:T(8,128)(2,1)} %hid_h.3, bf16[256,2048]{1,0:T(8,128)(2,1)} %wo_h.1), custom_call_target="tpu_custom_call" | custom-call | tf_op jit(solution)/shard_map/pallas_call | solution.py:675
  1.6 74.0 %shard_map.132 = (bf16[384,512]{1,0:T(8,128)(2,1)S(1)}, f32[2,384]{1,0:T(2,128)S(1)}) custom-call(bf16[4,384,512]{2,1,0:T(8,128)(2,1)} %get-tuple-element.6.hxe_h, bf16[1024,512]{1,0:T(8,128)(2,1)} %get-tuple-element.7.wce_h, bf16[384,512]{1,0:T(8,128)(2,1)} %hid_h.3, bf16[16,128]{1,0:T(8,128)(2,1)} %bitcast.3, bf16[2048,256]{1,0:T(8,128)(2,1)} %wq_h.1, ...), custom_call_target="tpu_custom_call" | custom-call | tf_op jit(solution)/shard_map/pallas_call | solution.py:692
  75.6 0.7 copy.16
  76.4 0.6 copy.17

commit v6 on v5

--- a/solution.py
+++ b/solution.py
@@ -525,21 +525,17 @@
 
     for c in range(NC):
         state[c] = x_near(c, x_pass(c))
-    pairs[0] = x_end(0, state[0])
-    pairs[1] = x_end(1, state[1])
-    pair_first(0)
-    pairs[2] = x_end(2, state[2])
-    pair_first(1)
-    pairs[3] = x_end(3, state[3])
-    pair_first(2)
+    for c in range(NC):
+        pairs[c] = x_end(c, state[c])
+        pair_first(c)
+    early(0)
     when(second, c_wc.wait)
     c_w = send(wcol, wcol, ws.at[0], wr.at[0], to_partner, second)
-    early(0)
     for c in range(3):
         pl.when(second)(functools.partial(own_pair, c, pairs[c]))
 
     pl.when(edge & second)(functools.partial(branch4, 0))
-    own_pair(3, pairs[3])
+    pl.when(second)(functools.partial(own_pair, 3, pairs[3]))
     for b in range(1, cj // 16):
         branch1(b)
     plans = [finish_plan(c) for c in range(NC)]

time: 77.1 us -> 76.6 us (level)
  no operation moved by 1% of the time
where the time goes in v6:
time: 76.6 us; the launch traced here: 76.4 us
  Pallas kernels  74.4 us (97%)
  local copies, waits for them, and re-layouts  1.33 us (2%)
    pallas_call x1, Pallas kernels, local(): pl.pallas_call(functools.partial(kernel, n_tp, n_sp), out_shape=(pltpu.VM...  73.4 us

profile of v6, /device:TPU:96, one launch (start us, length us, event | category | flops | bytes accessed | tf_op | source)
XLA Modules:
  0.0 76.4 jit_solution(6401396257499577608)
XLA Ops:
  0.6 1.0 %shard_map.131 = (bf16[4,384,512]{2,1,0:T(8,128)(2,1)}, bf16[1024,512]{1,0:T(8,128)(2,1)}) custom-call(bf16[384,512]{1,0:T(8,128)(2,1)} %hid_h.3, bf16[256,2048]{1,0:T(8,128)(2,1)} %wo_h.1), custom_call_target="tpu_custom_call" | custom-call | tf_op jit(solution)/shard_map/pallas_call | solution.py:671
  1.6 73.4 %shard_map.132 = (bf16[384,512]{1,0:T(8,128)(2,1)S(1)}, f32[2,384]{1,0:T(2,128)S(1)}) custom-call(bf16[4,384,512]{2,1,0:T(8,128)(2,1)} %get-tuple-element.6.hxe_h, bf16[1024,512]{1,0:T(8,128)(2,1)} %get-tuple-element.7.wce_h, bf16[384,512]{1,0:T(8,128)(2,1)} %hid_h.3, bf16[16,128]{1,0:T(8,128)(2,1)} %bitcast.3, bf16[2048,256]{1,0:T(8,128)(2,1)} %wq_h.1, ...), custom_call_target="tpu_custom_call" | custom-call | tf_op jit(solution)/shard_map/pallas_call | solution.py:688
  75.1 0.7 copy.16
  75.8 0.6 copy.17

commit v7 on v6

--- a/solution.py
+++ b/solution.py
@@ -223,7 +223,7 @@
     def _():
         with jax.named_scope("hid_wait"):
             c_hid.wait()
-        hx[me] = dot(perm, hid_v[...]).astype(BF)
+        hx[me, :rows, :] = dot(perm[:rows], hid_v[...]).astype(BF)
 
     with jax.named_scope("barrier_wait"):
         pl.semaphore_wait(barrier, len(peers) + has_up.astype(jnp.int32))
@@ -235,7 +235,13 @@
             send(part, part, xs_own.at[c, 1], xr_own.at[c, 1], to_lf, first),
         )
 
-    x_sent = {c: x_own(c) for c in range(NC)}
+    x_sent = {0: x_own(0)}
+
+    @pl.when(first)
+    def _():
+        hx[me, rows:, :] = dot(perm[rows:], hid_v[...]).astype(BF)
+
+    x_sent.update({c: x_own(c) for c in range(1, NC)})
 
     for stage, (lo, hi) in enumerate(((n_near, own0), (n_far, n_near), (0, n_far))):
         @pl.when(z <= stage)
@@ -504,11 +510,11 @@
         lhs = jnp.concatenate([ag[s, c, h] for s in range(n_tp) for h in range(2)], axis=1)
         mm[c * rows : (c + 1) * rows, :] = dot(lhs, wcol[...]).astype(BF)
 
-    t0 = iota((tok, rows), 0)
-    q0 = iota((tok, rows), 1)
+    t0 = iota((tok, 2 * rows), 0)
+    q0 = iota((tok, 2 * rows), 1)
 
     def back(c):
-        there = ((t0 & (NC - 1)) == c) & (q0 == ((t0 >> 2) & (NI - 1)) * nj + (t0 >> 4))
+        there = q0 + c * rows == (t0 & (NC - 1)) * rows + ((t0 >> 2) & (NI - 1)) * nj + (t0 >> 4)
         return jnp.where(there, 1.0, 0.0).astype(BF)
 
     state, pairs = {}, {}
@@ -576,11 +582,6 @@
     for c in range(1, NC - 1):
         a_fwd(c, fwd[c])
     fwd[NC - 1] = ()
-    with jax.named_scope("w_wait"):
-        when(first, c_w.wait_recv)
-    for c in range(3):
-        a_mix(c, fwd[c])
-    macc[...] = sum(dot(back(c), mm[c * rows : (c + 1) * rows, :]) for c in range(3))
     for c in range(NC):
         plans[c][-1].wait_recv()
     lane = iota((1, hd), 1)
@@ -594,8 +595,14 @@
         p = perm[c * rows : (c + 1) * rows, :]
         acc = acc + (dot_tn(hi, p) + dot_tn(mid, p) + dot_tn(low, p))
     log_ref[...] = acc[:2, :]
+    with jax.named_scope("w_wait"):
+        when(first, c_w.wait_recv)
+    a_mix(0, fwd[0])
+    a_mix(1, fwd[1])
+    macc[...] = dot(back(0), mm[: 2 * rows, :])
+    a_mix(2, fwd[2])
     a_mix(3, fwd[3])
-    out_ref[...] = (macc[...] + dot(back(3), mm[3 * rows :, :])).astype(BF)
+    out_ref[...] = (macc[...] + dot(back(2), mm[2 * rows :, :])).astype(BF)
     with jax.named_scope("drain"):
         for cond, copy in pending:
             when(cond, copy.wait_send)

time: 76.6 us -> 75.9 us (level)
  no operation moved by 1% of the time
where the time goes in v7:
time: 75.9 us; the launch traced here: 75.7 us
  Pallas kernels  73.8 us (97%)
  local copies, waits for them, and re-layouts  1.33 us (2%)
    pallas_call x1, Pallas kernels, local(): pl.pallas_call(functools.partial(kernel, n_tp, n_sp), out_shape=(pltpu.VM...  72.8 us

profile of v7, /device:TPU:96, one launch (start us, length us, event | category | flops | bytes accessed | tf_op | source)
XLA Modules:
  0.0 75.7 jit_solution(292244318207039592)
XLA Ops:
  0.6 1.0 %shard_map.131 = (bf16[4,384,512]{2,1,0:T(8,128)(2,1)}, bf16[1024,512]{1,0:T(8,128)(2,1)}) custom-call(bf16[384,512]{1,0:T(8,128)(2,1)} %hid_h.3, bf16[256,2048]{1,0:T(8,128)(2,1)} %wo_h.1), custom_call_target="tpu_custom_call" | custom-call | tf_op jit(solution)/shard_map/pallas_call | solution.py:678
  1.6 72.8 %shard_map.132 = (bf16[384,512]{1,0:T(8,128)(2,1)S(1)}, f32[2,384]{1,0:T(2,128)S(1)}) custom-call(bf16[4,384,512]{2,1,0:T(8,128)(2,1)} %get-tuple-element.6.hxe_h, bf16[1024,512]{1,0:T(8,128)(2,1)} %get-tuple-element.7.wce_h, bf16[384,512]{1,0:T(8,128)(2,1)} %hid_h.3, bf16[16,128]{1,0:T(8,128)(2,1)} %bitcast.3, bf16[2048,256]{1,0:T(8,128)(2,1)} %wq_h.1, ...), custom_call_target="tpu_custom_call" | custom-call | tf_op jit(solution)/shard_map/pallas_call | solution.py:695
  74.4 0.7 copy.16
  75.2 0.6 copy.17
